TPU v7x, 1024 devices: a whole 8x8x8 slice. The times are simulated.
1024 devices in a mesh: sp: 16 (over x, core), dp: 64 (over z, y).
Axes of the slice: x: 8, y: 8, z: 8, core: 2. Of those that a mesh axis runs over, the one named last changes fastest.
Arguments:
- content_features_raw: bfloat16 [64, 2048, 3072], P('dp', 'sp'), may hold values from -6 to 6
- memory_entering_matrix: bfloat16 [64, 2048, 2048], P('dp', 'sp'), may hold values from -6 to 6
- memory_leaving_matrix: bfloat16 [64, 2048, 2048], P('dp', 'sp'), may hold values from -6 to 6
- feature_switch_signal: bfloat16 [64, 2048, 3072], P('dp', 'sp'), may hold values from -6 to 6
- ahead_increment_raw: float32 [64, 2048, 48], P('dp', 'sp'), may hold values from -5 to 5
- reverse_increment_raw: float32 [64, 2048, 48], P('dp', 'sp'), may hold values from -5 to 5
- additional_fading: float32 [64, 2048, 48], P('dp', 'sp'), as said below
- content_filter_weights: bfloat16 [4, 3072], P(None, 'sp'), may hold values from -3 to 3
- entering_filter_weights: bfloat16 [4, 2048], P(None, 'sp'), may hold values from -3 to 3
- leaving_filter_weights: bfloat16 [4, 2048], P(None, 'sp'), may hold values from -3 to 3
- increment_offset_lanes: float32 [2, 48], P(None, 'sp'), may hold values from -0.5 to 0.5
- fading_speed_exponents: float32 [2, 48], P(None, 'sp'), as said below
- result_scaling_factor: bfloat16 [3072], replicated, may hold values from 0.099609375 to 1.8984375
Outputs:
- out: bfloat16 [64, 2048, 3072], P('dp', 'sp')
Inputs may be any that keep to these rules, and one draw needn't show every extreme that they name: Each head's row has a rate exp(fading_speed_exponents) between 0.3 / 131072 and 0.05. `additional_fading`: zero at most positions; elsewhere between log(0.5) and log(0.8).
All inputs are finite; a program needn't handle non-finite values.
Results may differ from a plain program's by a relative error of at most 0.0051.
Values may be sent and summed in bfloat16 or wider, within the bound.
A program may use at most 64 MiB of HBM per device.

v0:
```python
import functools

import jax
import jax.numpy as jnp
from jax import lax
from jax.experimental import pallas as pl
from jax.experimental.pallas import tpu as pltpu
from jax.sharding import Mesh
from jax.sharding import PartitionSpec as P

MESH = pl.DeviceIdType.MESH
HEAD_DIM = 64
STATE = 128
TOK = 128
HPG = 3
GW = HPG * HEAD_DIM
PW = 2 * GW
HIGH = lax.Precision.HIGHEST
F32 = jnp.float32
BF16 = jnp.bfloat16


def iota(shape, dim):
    return lax.broadcasted_iota(jnp.int32, shape, dim)


def mm(a, b, precision=None):
    return jnp.dot(a, b, preferred_element_type=F32, precision=precision)


def rcopy(src, dst, send_sem, recv_sem, device):
    return pltpu.make_async_remote_copy(
        src_ref=src,
        dst_ref=dst,
        send_sem=send_sem,
        recv_sem=recv_sem,
        device_id=device,
        device_id_type=MESH,
    )


def expand(columns, ids):
    low = iota((columns.shape[0], 128), 1) < HEAD_DIM
    pieces = []
    for v in range(len(ids) // 2):
        a, b = ids[2 * v], ids[2 * v + 1]
        pieces.append(jnp.where(low, columns[:, a : a + 1], columns[:, b : b + 1]))
    return jnp.concatenate(pieces, axis=1)


def group_ids(q):
    return [HPG * q + i for i in range(HPG)] + [8 + HPG * q + i for i in range(HPG)]


def conv_silu(own, other, before, after, taps, first):
    own, other = own.astype(F32), other.astype(F32)
    x = jnp.concatenate(
        [jnp.where(first, own, other), jnp.where(first, other, own)], axis=0
    )
    rows = x.shape[0]
    row = iota(x.shape, 0)
    m1 = jnp.where(row == 0, before[1:2], pltpu.roll(x, 1, 0))
    m2 = jnp.where(
        row == 0, before[0:1], jnp.where(row == 1, before[1:2], pltpu.roll(x, 2, 0))
    )
    p1 = jnp.where(row == rows - 1, after[0:1], pltpu.roll(x, rows - 1, 0))
    total = m2 * taps[0:1] + m1 * taps[1:2] + x * taps[2:3] + p1 * taps[3:4]
    return (total / (1.0 + jnp.exp(-total))).astype(BF16)


def kernel(
    sizes,
    x_ref, b_ref, c_ref, z_ref, ra_ref, rr_ref, rf_ref,
    wx_ref, wb_ref, wc_ref, off_ref, spd_ref, gain_ref,
    out_ref,
    xo, bo, co, ro, hs, hr, ws, wr,
    cum_t, rate_t, fac_t, ecum_t,
    xc, bc, cc, yl,
    ts, tr, ls, lr, pre, pcl,
    ss, sl, yr, ylr, ypre, ypcl,
    zq, zql, zr, zlr,
    isd, ir, es, er,
    ys, yx,
    d_s, d_r, h_s, h_r, w_s, w_r,
    t_s, t_r, l_s, l_r, s_s, s_r, sl_s, sl_r,
    q_s, q_r, ql_s, ql_r, i_s, i_r, e_s, e_r, y_s, y_r,
):
    nx, ny, nz = sizes
    pairs = nx // 2
    xw, bw = pairs * PW, pairs * 2 * STATE
    x, c, z, y = (lax.axis_index(n) for n in ("x", "c", "z", "y"))
    first = c == 0
    partner = {"c": 1 - c}
    lin = (z * ny + y) * nx + x
    total_chips = nx * ny * nz
    has_prev, has_next = lin > 0, lin < total_chips - 1

    def chip(at):
        at = lax.rem(at + total_chips, total_chips)
        rest = at // nx
        return {"x": lax.rem(at, nx), "y": lax.rem(rest, ny), "z": rest // ny}

    target_exists = jnp.logical_or(
        jnp.logical_and(first, has_prev), jnp.logical_and(jnp.logical_not(first), has_next)
    )
    target = chip(jnp.where(first, lin - 1, lin + 1))

    barrier = pltpu.get_barrier_semaphore()

    def greet(device):
        pl.semaphore_signal(barrier, inc=1, device_id=device, device_id_type=MESH)

    greet(partner)

    @pl.loop(1, nx)
    def _(k):
        at = lax.rem(x + k, nx)
        greet({"x": at})
        greet({"x": at, "c": 1 - c})

    @pl.loop(1, ny)
    def _(k):
        greet({"y": lax.rem(y + k, ny)})

    @pl.loop(1, nz)
    def _(k):
        greet({"z": lax.rem(z + k, nz)})

    @pl.when(has_prev)
    def _():
        greet({**chip(lin - 1), "c": 1})

    @pl.when(has_next)
    def _():
        greet({**chip(lin + 1), "c": 0})

    group = 2 * x + c
    slot = lax.rem(group, nx)
    parity = lax.rem(slot, 2)
    place = (iota((GW, PW), 1) == iota((GW, PW), 0) + GW * parity).astype(BF16)
    ws[0:4, 0:PW] = mm(wx_ref[...], place)
    ws[0:4, PW : PW + STATE] = wb_ref[...].astype(F32)
    ws[0:4, PW + STATE : PW + 2 * STATE] = wc_ref[...].astype(F32)
    lane = iota((1, 128), 1)
    base = 16 * (slot // 2) + HPG * parity
    offsets = jnp.zeros((1, 128), F32)
    speeds = jnp.zeros((1, 128), F32)
    for d in range(2):
        for i in range(HPG):
            here = lane == base + 8 * d + i
            offsets = jnp.where(here, off_ref[d : d + 1, i : i + 1], offsets)
            speeds = jnp.where(here, spd_ref[d : d + 1, i : i + 1], speeds)
    ws[4:5, 0:128] = offsets
    ws[5:6, 0:128] = speeds

    at = 0
    for ref, width in ((x_ref, xw), (b_ref, bw), (c_ref, bw)):
        for half in range(2):
            cols = pl.ds(half * width, width)
            last = ref[0, TOK - 16 : TOK, cols].astype(F32)[8:16]
            start = ref[0, 0:16, cols].astype(F32)[0:8]
            rows = jnp.where(first, start, pltpu.roll(last, 2, 0))
            hs[half, :, at : at + width] = rows[0:2]
        at += width

    @pl.when(jnp.logical_not(has_prev))
    def _():
        hr[0] = jnp.zeros(hr.shape[1:], F32)

    @pl.when(jnp.logical_not(has_next))
    def _():
        hr[1] = jnp.zeros(hr.shape[1:], F32)

    expected = 1 + 2 * (nx - 1) + (ny - 1) + (nz - 1)
    pl.semaphore_wait(barrier, expected + jnp.where(target_exists, 2, 0))

    def half_of(ref, width, half):
        return ref.at[0, :, pl.ds(pl.multiple_of(half * width, 128), width)]

    rate_copies = [
        rcopy(ref.at[0], ro.at[k], d_s.at[k], d_r.at[k], partner)
        for k, ref in enumerate((ra_ref, rr_ref, rf_ref))
    ]
    data_copies = [
        rcopy(half_of(ref, width, 1 - c), dst, d_s.at[3 + k], d_r.at[3 + k], partner)
        for k, (ref, width, dst) in enumerate(((x_ref, xw, xo), (b_ref, bw, bo), (c_ref, bw, co)))
    ]
    for copy in rate_copies:
        copy.start()

    to_core = group // nx

    def weight_copy(j):
        return rcopy(ws, wr.at[slot], w_s.at[j], w_r.at[slot], {"x": j, "c": to_core})

    def weight_is_mine(j):
        return jnp.logical_and(j == x, to_core == c)

    @pl.loop(0, nx)
    def _(k):
        j = lax.rem(x + k, nx)

        @pl.when(jnp.logical_not(weight_is_mine(j)))
        def _():
            weight_copy(j).start()

    @pl.when(to_core == c)
    def _():
        wr[slot] = ws[...]

    def halo_copy(half):
        return rcopy(
            hs.at[half], hr.at[1 - c], h_s.at[half], h_r.at[1 - c], {**target, "c": half}
        )

    @pl.when(target_exists)
    def _():
        for half in range(2):
            halo_copy(half).start()

    for copy in data_copies:
        copy.start()

    for copy in rate_copies:
        copy.wait_recv()

    @pl.loop(0, nx)
    def _(j):
        @pl.when(jnp.logical_not(nx * c + j == group))
        def _():
            rcopy(ws, wr.at[j], w_s.at[j], w_r.at[j], partner).wait_recv()

    heads = ra_ref.shape[2]
    head, lanes = iota((heads, 128), 0), iota((heads, 128), 1)
    pair, rest = lanes // 16, lax.rem(lanes, 16)
    inside = lax.rem(rest, 8)
    valid = jnp.logical_and(inside < 6, pair < pairs)
    valid = jnp.logical_and(valid, head == 6 * pairs * c + 6 * pair + inside)
    pick_f = jnp.logical_and(valid, rest < 8).astype(F32)
    pick_b = jnp.logical_and(valid, rest >= 8).astype(F32)

    def both(ref, k):
        own, other = ref[0], ro[k]
        return jnp.concatenate(
            [jnp.where(first, own, other), jnp.where(first, other, own)], axis=0
        )

    raw = mm(both(ra_ref, 0), pick_f, HIGH) + mm(both(rr_ref, 1), pick_b, HIGH)
    fading = mm(both(rf_ref, 2), pick_f + pick_b, HIGH)
    offset_row = wr[0, 4:5, 0:128]
    speed_row = wr[0, 5:6, 0:128]
    for j in range(1, nx):
        offset_row = offset_row + wr[j, 4:5, 0:128]
        speed_row = speed_row + wr[j, 5:6, 0:128]
    pre_rate = raw + offset_row
    rate = jnp.maximum(pre_rate, 0.0) + jnp.log1p(jnp.exp(-jnp.abs(pre_rate)))
    log = fading - jnp.exp(speed_row) * rate
    n = 2 * TOK
    row_i, col_i = iota((n, n), 0), iota((n, n), 1)
    forward = lax.rem(iota((1, 128), 1), 16) < 8
    cum = jnp.where(
        forward,
        mm((col_i <= row_i).astype(F32), log, HIGH),
        mm((col_i >= row_i).astype(F32), log, HIGH),
    )
    span = jnp.where(forward, cum[n - 1 : n], cum[0:1])
    cum_t[...] = cum.T
    rate_t[...] = rate.T
    fac_t[...] = (rate * jnp.exp(span - cum)).T
    ecum_t[...] = jnp.exp(cum).T

    @pl.when(has_prev)
    def _():
        rcopy(hs.at[0], hr.at[0], h_s.at[0], h_r.at[0], partner).wait_recv()

    @pl.when(has_next)
    def _():
        rcopy(hs.at[0], hr.at[1], h_s.at[0], h_r.at[1], partner).wait_recv()

    for copy in data_copies:
        copy.wait_recv()

    half_lane = iota((1, PW), 1) < GW

    def rows_of(p):
        return pl.ds(pl.multiple_of(16 * p, 16), 16)

    def x_cols(p):
        return pl.ds(pl.multiple_of(PW * p, 128), PW)

    def b_cols(p):
        return pl.ds(pl.multiple_of(2 * STATE * p, 128), 2 * STATE)

    def state_copy(j):
        return rcopy(ts.at[j], tr.at[x], t_s.at[j], t_r.at[x], {"x": j})

    def log_copy(j):
        return rcopy(ls.at[j], lr.at[x], l_s.at[j], l_r.at[x], {"x": j})

    @pl.loop(0, pairs)
    def _(k):
        p = lax.rem(x // 2 + 1 + k, pairs)
        w0, w1 = wr[2 * p], wr[2 * p + 1]
        cols, start = x_cols(p), pl.multiple_of(PW * p, 128)
        x_cols_in = pl.ds(pl.multiple_of(c * xw + start, 128), PW)
        xv = conv_silu(
            x_ref[0, :, x_cols_in], xo[:, cols], hr[0, :, cols], hr[1, :, cols],
            w0[0:4, 0:PW] + w1[0:4, 0:PW], first,
        )
        xc[:, cols] = xv
        convs = []
        for own, other, dst, at, lo in ((b_ref, bo, bc, xw, PW), (c_ref, co, cc, xw + bw, PW + STATE)):
            start = pl.multiple_of(2 * STATE * p, 128)
            taps = jnp.concatenate([w0[0:4, lo : lo + STATE], w1[0:4, lo : lo + STATE]], axis=1)
            cols_in = pl.ds(pl.multiple_of(c * bw + start, 128), 2 * STATE)
            cols_h = pl.ds(pl.multiple_of(at + start, 128), 2 * STATE)
            v = conv_silu(
                own[0, :, cols_in], other[:, b_cols(p)], hr[0, :, cols_h], hr[1, :, cols_h],
                taps, first,
            )
            dst[:, b_cols(p)] = v
            convs.append(v)
        factors = fac_t[rows_of(p)].T
        cums = cum_t[rows_of(p)].T
        direction = iota((1, 16), 1) < 8
        spans = jnp.where(direction, cums[n - 1 : n], cums[0:1])
        xf = xv.astype(F32)
        swapped = pltpu.roll(xf, GW, 1)
        bf = convs[0].astype(F32)
        for q in range(2):
            j = 2 * p + q
            twice = jnp.where(half_lane, xf, swapped) if q == 0 else jnp.where(half_lane, swapped, xf)
            scaled = twice * expand(factors, group_ids(q))
            hi = scaled.astype(BF16)
            lo = (scaled - hi.astype(F32)).astype(BF16)
            bt = bf[:, q * STATE : (q + 1) * STATE].T.astype(BF16)
            update = (mm(bt, hi) + mm(bt, lo)).astype(BF16)
            span_row = expand(spans, group_ids(q))

            @pl.when(j == x)
            def _():
                tr[x] = update
                lr[x] = span_row

            @pl.when(j != x)
            def _():
                ls[j] = span_row
                ts[j] = update
                log_copy(j).start()
                state_copy(j).start()

    @pl.loop(0, pairs)
    def _(p):
        cum_r, rate_r = cum_t[rows_of(p)], rate_t[rows_of(p)]
        cum_c = cum_r.T
        xv, bv, cv = xc[:, x_cols(p)], bc[:, b_cols(p)], cc[:, b_cols(p)]
        below, above = col_i < row_i, col_i > row_i
        low = iota((n, 128), 1) < HEAD_DIM
        products = []
        for q in range(2):
            scores = lax.dot_general(
                cv[:, q * STATE : (q + 1) * STATE], bv[:, q * STATE : (q + 1) * STATE],
                (((1,), (1,)), ((), ())), preferred_element_type=F32,
            )
            for i in range(HPG):
                f, g = HPG * q + i, 8 + HPG * q + i
                gap = jnp.where(
                    above,
                    cum_c[:, g : g + 1] - cum_r[g : g + 1],
                    cum_c[:, f : f + 1] - cum_r[f : f + 1],
                )
                r_f, r_b = rate_r[f : f + 1], rate_r[g : g + 1]
                coef = jnp.where(below, r_f, jnp.where(above, r_b, r_f + r_b))
                weights = (scores * jnp.exp(gap) * coef).astype(BF16)
                v = f // 2
                products.append(mm(weights, xv[:, 128 * v : 128 * (v + 1)]))
        yl[:, x_cols(p)] = jnp.concatenate(
            [jnp.where(low, products[2 * v], products[2 * v + 1]) for v in range(HPG)], axis=1
        )

    @pl.loop(0, nx)
    def _(k):
        @pl.when(k != x)
        def _():
            rcopy(ls.at[k], lr.at[k], l_s.at[k], l_r.at[k], partner).wait_recv()
            rcopy(ts.at[k], tr.at[k], t_s.at[k], t_r.at[k], partner).wait_recv()

    pre[0] = jnp.zeros(pre.shape[1:], F32)
    pcl[0] = jnp.zeros(pcl.shape[1:], F32)

    @pl.loop(0, nx)
    def _(k):
        d = jnp.where(half_lane, lr[k], lr[nx - 1 - k])
        v = jnp.where(half_lane, tr[k], tr[nx - 1 - k]).astype(F32)
        pre[k + 1] = pre[k] * jnp.exp(d) + v
        pcl[k + 1] = pcl[k] + d

    ry = STATE // ny

    def y_rows(j):
        return pl.ds(pl.multiple_of(ry * j, ry), ry)

    ss[...] = pre[nx].astype(ss.dtype)
    sl[...] = pcl[nx]

    @pl.loop(1, ny)
    def _(k):
        j = lax.rem(y + k, ny)
        rcopy(sl, ylr.at[y], sl_s.at[j], sl_r.at[y], {"y": j}).start()
        rcopy(ss.at[y_rows(j)], yr.at[y], s_s.at[j], s_r.at[y], {"y": j}).start()

    yr[y] = ss[y_rows(y)]
    ylr[y] = sl[...]

    @pl.loop(1, ny)
    def _(k):
        j = lax.rem(y + k, ny)
        rcopy(sl, ylr.at[j], sl_s.at[j], sl_r.at[j], {"y": j}).wait_recv()
        rcopy(ss.at[y_rows(j)], yr.at[j], s_s.at[j], s_r.at[j], {"y": j}).wait_recv()

    ypre[0] = jnp.zeros(ypre.shape[1:], F32)
    ypcl[0] = jnp.zeros(ypcl.shape[1:], F32)

    @pl.loop(0, ny)
    def _(k):
        d = jnp.where(half_lane, ylr[k], ylr[ny - 1 - k])
        v = jnp.where(half_lane, yr[k].astype(F32), yr[ny - 1 - k].astype(F32))
        ypre[k + 1] = ypre[k] * jnp.exp(d) + v
        ypcl[k + 1] = ypcl[k] + d

    zq[...] = ypre[ny]
    zql[...] = ypcl[ny]

    @pl.loop(1, nz)
    def _(k):
        j = lax.rem(z + k, nz)
        rcopy(zql, zlr.at[z], ql_s.at[j], ql_r.at[z], {"z": j}).start()
        rcopy(zq, zr.at[z], q_s.at[j], q_r.at[z], {"z": j}).start()

    zr[z] = zq[...]
    zlr[z] = zql[...]

    @pl.loop(1, nz)
    def _(k):
        j = lax.rem(z + k, nz)
        rcopy(zql, zlr.at[j], ql_s.at[j], ql_r.at[j], {"z": j}).wait_recv()
        rcopy(zq, zr.at[j], q_s.at[j], q_r.at[j], {"z": j}).wait_recv()

    running = jnp.zeros((ry, PW), F32)
    entering = jnp.zeros((ry, PW), F32)
    wanted = jnp.where(half_lane, z, nz - 1 - z)
    for k in range(nz):
        entering = jnp.where(wanted == k, running, entering)
        d = jnp.where(half_lane, zlr[k], zlr[nz - 1 - k])
        v = jnp.where(half_lane, zr[k], zr[nz - 1 - k])
        running = running * jnp.exp(d) + v

    def incoming(k):
        return ypre[k] + jnp.exp(ypcl[k]) * entering

    @pl.loop(1, ny)
    def _(k):
        j = lax.rem(y + k, ny)
        isd[j] = jnp.where(half_lane, incoming(j), incoming(ny - 1 - j)).astype(isd.dtype)
        rcopy(isd.at[j], ir.at[y_rows(y)], i_s.at[j], i_r.at[y], {"y": j}).start()

    ir[y_rows(y)] = jnp.where(half_lane, incoming(y), incoming(ny - 1 - y)).astype(ir.dtype)

    @pl.loop(1, ny)
    def _(k):
        j = lax.rem(y + k, ny)
        rcopy(isd.at[j], ir.at[y_rows(j)], i_s.at[j], i_r.at[j], {"y": j}).wait_recv()

    def entry(j):
        here = ir[...].astype(F32)
        f = pre[j] + jnp.exp(pcl[j]) * here
        b = pre[nx - 1 - j] + jnp.exp(pcl[nx - 1 - j]) * here
        return jnp.where(half_lane, f, b).astype(BF16)

    @pl.loop(1, nx)
    def _(k):
        j = lax.rem(x + k, nx)
        es[j] = entry(j)
        rcopy(es.at[j], er.at[x], e_s.at[j], e_r.at[x], {"x": j}).start()

    er[x] = entry(x)

    block_r, block_c = iota((128, 128), 0) // HEAD_DIM, iota((128, 128), 1) // HEAD_DIM
    ones = (block_r == block_c).astype(BF16)

    def gate(mixed, cols):
        zz = z_ref[0, :, cols].astype(F32)
        g = mixed.astype(F32) * (zz / (1.0 + jnp.exp(-zz)))
        sq = g * g
        hi = sq.astype(BF16)
        lo = (sq - hi.astype(F32)).astype(BF16)
        means = jnp.concatenate(
            [
                mm(hi[:, 128 * v : 128 * (v + 1)], ones) + mm(lo[:, 128 * v : 128 * (v + 1)], ones)
                for v in range(HPG)
            ],
            axis=1,
        ) * (1.0 / HEAD_DIM)
        normed = g * lax.rsqrt(means + 1e-06)
        out_ref[0, :, cols] = (normed * gain_ref[:, cols].astype(F32)).astype(BF16)

    def own_cols(p, half):
        return pl.ds(pl.multiple_of(half * xw + PW * p, 128), PW)

    def mixed_copy(p):
        return rcopy(ys.at[p], yx.at[p], y_s.at[p], y_r.at[p], partner)

    @pl.loop(0, pairs)
    def _(k):
        p = lax.rem(x // 2 + k, pairs)
        cv = cc[:, b_cols(p)]
        decays = ecum_t[rows_of(p)].T
        carried = []
        for q in range(2):
            j = 2 * p + q

            @pl.when(j != x)
            def _():
                rcopy(es.at[j], er.at[j], e_s.at[j], e_r.at[j], partner).wait_recv()

            v = mm(cv[:, q * STATE : (q + 1) * STATE], er[j]) * expand(decays, group_ids(q))
            carried.append(v + pltpu.roll(v, GW, 1))
        mixed = yl[:, x_cols(p)] + jnp.where(half_lane, carried[0], carried[1])
        top, bottom = mixed[0:TOK].astype(BF16), mixed[TOK:n].astype(BF16)
        ys[p] = jnp.where(first, bottom, top)
        mixed_copy(p).start()
        gate(jnp.where(first, top, bottom), own_cols(p, c))

    @pl.loop(0, pairs)
    def _(k):
        p = lax.rem((x // 2) + k, pairs)
        mixed_copy(p).wait_recv()
        gate(yx[p], own_cols(p, 1 - c))

    for copy in rate_copies + data_copies:
        copy.wait_send()

    @pl.when(target_exists)
    def _():
        for half in range(2):
            halo_copy(half).wait_send()

    @pl.loop(0, nx)
    def _(j):
        @pl.when(jnp.logical_not(weight_is_mine(j)))
        def _():
            weight_copy(j).wait_send()

        @pl.when(j != x)
        def _():
            log_copy(j).wait_send()
            state_copy(j).wait_send()
            rcopy(es.at[j], er.at[x], e_s.at[j], e_r.at[x], {"x": j}).wait_send()

    @pl.loop(1, ny)
    def _(k):
        j = lax.rem(y + k, ny)
        rcopy(sl, ylr.at[y], sl_s.at[j], sl_r.at[y], {"y": j}).wait_send()
        rcopy(ss.at[y_rows(j)], yr.at[y], s_s.at[j], s_r.at[y], {"y": j}).wait_send()
        rcopy(isd.at[j], ir.at[y_rows(y)], i_s.at[j], i_r.at[y], {"y": j}).wait_send()

    @pl.loop(1, nz)
    def _(k):
        j = lax.rem(z + k, nz)
        rcopy(zql, zlr.at[z], ql_s.at[j], ql_r.at[z], {"z": j}).wait_send()
        rcopy(zq, zr.at[z], q_s.at[j], q_r.at[z], {"z": j}).wait_send()

    @pl.loop(0, pairs)
    def _(p):
        mixed_copy(p).wait_send()


def local(sizes, *args):
    nx, ny, nz = sizes
    pairs = nx // 2
    xw, bw = pairs * PW, pairs * 2 * STATE
    n = 2 * TOK
    ry = STATE // ny
    args = args[:-1] + (args[-1][None],)
    dma = pltpu.SemaphoreType.DMA
    vmem = pltpu.VMEM
    scratch = [
        vmem((TOK, xw), BF16), vmem((TOK, bw), BF16), vmem((TOK, bw), BF16),
        vmem((3, TOK, args[4].shape[2]), F32),
        vmem((2, 2, xw + 2 * bw), F32), vmem((2, 2, xw + 2 * bw), F32),
        vmem((8, PW + 2 * STATE), F32), vmem((nx, 8, PW + 2 * STATE), F32),
        vmem((128, n), F32), vmem((128, n), F32), vmem((128, n), F32), vmem((128, n), F32),
        vmem((n, xw), BF16), vmem((n, bw), BF16), vmem((n, bw), BF16), vmem((n, xw), F32),
        vmem((nx, STATE, PW), BF16), vmem((nx, STATE, PW), BF16),
        vmem((nx, 1, PW), F32), vmem((nx, 1, PW), F32),
        vmem((nx + 1, STATE, PW), F32), vmem((nx + 1, 1, PW), F32),
        vmem((STATE, PW), BF16), vmem((1, PW), F32),
        vmem((ny, ry, PW), BF16), vmem((ny, 1, PW), F32),
        vmem((ny + 1, ry, PW), F32), vmem((ny + 1, 1, PW), F32),
        vmem((ry, PW), F32), vmem((1, PW), F32),
        vmem((nz, ry, PW), F32), vmem((nz, 1, PW), F32),
        vmem((ny, ry, PW), BF16), vmem((STATE, PW), BF16),
        vmem((nx, STATE, PW), BF16), vmem((nx, STATE, PW), BF16),
        vmem((pairs, TOK, PW), BF16), vmem((pairs, TOK, PW), BF16),
    ]
    counts = [6, 6, 2, 2, nx, nx, nx, nx, nx, nx, ny, ny, ny, ny, nz, nz, nz, nz, ny, ny, nx, nx, pairs, pairs]
    scratch += [dma((k,)) for k in counts]
    return pl.pallas_call(
        functools.partial(kernel, sizes),
        out_shape=jax.ShapeDtypeStruct(args[0].shape, BF16),
        in_specs=[pl.BlockSpec(memory_space=pltpu.VMEM)] * len(args),
        out_specs=pl.BlockSpec(memory_space=pltpu.VMEM),
        scratch_shapes=scratch,
        compiler_params=pltpu.CompilerParams(
            collective_id=0, has_side_effects=True, vmem_limit_bytes=60 * 1024 * 1024
        ),
        name="mixer",
    )(*args)


def solution(mesh):
    sp, dp = mesh.shape["sp"], mesh.shape["dp"]
    nx = sp // 2
    ny = max(k for k in range(1, dp + 1) if dp % k == 0 and k * k <= dp)
    nz = dp // ny
    torus = Mesh(mesh.devices.reshape(nx, 2, nz, ny), ("x", "c", "z", "y"))
    rows = P(("z", "y"), ("x", "c"), None)
    cols = P(None, ("x", "c"))
    return jax.shard_map(
        functools.partial(local, (nx, ny, nz)),
        mesh=torus,
        in_specs=(rows,) * 7 + (cols,) * 5 + (P(),),
        out_specs=rows,
        check_vma=False,
    )
```

profile of v0, /device:TPU:1, one launch (start us, length us, event | category | flops | bytes accessed | tf_op | source)
XLA Modules:
  0.0 102.1 jit_solution(1478360182966475968)
XLA Ops:
  0.0 1.3 %broadcast_in_dim.3.gain_ref = bf16[1,3072]{1,0:T(2,128)(2,1)} reshape(bf16[3072]{0:T(1024)(128)(2,1)} %param.25) | data formatting | bytes 12288 | tf_op jit(solution)/shard_map/broadcast_in_dim | solution.py:584
  1.3 0.0 copy-start
  1.3 1.5 %copy.14.ra_ref = f32[1,128,48]{2,1,0:T(8,128)} copy(f32[1,128,48]{1,2,0:T(8,128)} %param.17) | data formatting | bytes 49152 | tf_op args[4]
  2.8 0.0 copy-done
  2.8 0.0 copy-start.1
  2.8 0.7 copy.15.rr_ref
  3.5 0.0 copy-done.1
  3.5 0.7 copy.16.rf_ref
  4.2 95.8 %mixer.1 = bf16[1,128,3072]{2,1,0:T(8,128)(2,1)} custom-call(bf16[1,128,3072]{2,1,0:T(8,128)(2,1)} %x_ref.1, bf16[1,128,2048]{2,1,0:T(8,128)(2,1)} %b_ref.1, bf16[1,128,2048]{2,1,0:T(8,128)(2,1)} %c_ref.1, bf16[1,128,3072]{2,1,0:T(8,128)(2,1)} %z_ref.1, f32[1,128,48]{2,1,0:T(8,128)} %copy.14.ra_ref, f32[1,128,48]{2,1,0:T(8,128)} %copy.15.rr_ref, ...), custom_call_target="tpu_custom_call" | custom-call | tf_op jit(solution)/shard_map/mixer/pallas_call | solution.py:608
  100.0 2.1 %copy.18 = bf16[1,128,3072]{2,1,0:T(8,128)(2,1)} copy(bf16[1,128,3072]{2,1,0:T(8,128)(2,1)} %mixer.1) | data formatting | bytes 1572864
Async XLA Ops:
  1.3 1.5 %copy-start = (f32[1,128,48]{1,2,0:T(8,128)S(1)}, f32[1,128,48]{1,2,0:T(8,128)}, u32[]{:S(2)}) copy-start(f32[1,128,48]{1,2,0:T(8,128)} %param.18) | copy-start | bytes 73732
  2.8 0.7 copy-start.1
where the time goes:
time: 102 us
  Pallas kernels  95.8 us (94%)
  local copies, waits for them, and re-layouts  6.29 us (6%)
    pallas_call x1, Pallas kernels, local(): pl.pallas_call(functools.partial(kernel, sizes), out_shape=jax.ShapeDtype...  95.8 us
    unnamed x8, local copies, waits for them, and re-layouts  5 us

commit v1 on v0

v1 whole, which is shorter than its diff:
```python
import functools

import jax
import jax.numpy as jnp
from jax import lax
from jax.experimental import pallas as pl
from jax.experimental.pallas import tpu as pltpu
from jax.sharding import Mesh
from jax.sharding import PartitionSpec as P

MESH = pl.DeviceIdType.MESH
HEAD_DIM = 64
STATE = 128
TOK = 128
HPG = 3
TAPS = 4
GW = HPG * HEAD_DIM
PW = 2 * GW
HIGH = lax.Precision.HIGHEST
F32 = jnp.float32
BF16 = jnp.bfloat16


def iota(shape, dim):
    return lax.broadcasted_iota(jnp.int32, shape, dim)


def mm(a, b, precision=None):
    return jnp.dot(a, b, preferred_element_type=F32, precision=precision)


def rcopy(src, dst, send_sem, recv_sem, device):
    return pltpu.make_async_remote_copy(
        src_ref=src,
        dst_ref=dst,
        send_sem=send_sem,
        recv_sem=recv_sem,
        device_id=device,
        device_id_type=MESH,
    )


def head_rows(columns, f, b):
    low = iota((columns.shape[0], 128), 1) < HEAD_DIM
    return jnp.where(low, columns[:, f : f + 1], columns[:, b : b + 1])


def conv_silu(own, other, before, after, taps, first):
    own, other = own.astype(F32), other.astype(F32)
    x = jnp.concatenate(
        [jnp.where(first, own, other), jnp.where(first, other, own)], axis=0
    )
    rows = x.shape[0]
    row = iota(x.shape, 0)
    m1 = jnp.where(row == 0, before[1:2], pltpu.roll(x, 1, 0))
    m2 = jnp.where(
        row == 0, before[0:1], jnp.where(row == 1, before[1:2], pltpu.roll(x, 2, 0))
    )
    p1 = jnp.where(row == rows - 1, after[0:1], pltpu.roll(x, rows - 1, 0))
    total = m2 * taps[0:1] + m1 * taps[1:2] + x * taps[2:3] + p1 * taps[3:4]
    return (total / (1.0 + jnp.exp(-total))).astype(BF16)


def three(v):
    hi = v.astype(BF16)
    left = v - hi.astype(F32)
    mid = left.astype(BF16)
    return hi, mid, (left - mid.astype(F32)).astype(BF16)


def kernel(
    sizes,
    x_ref, b_ref, c_ref, z_ref, ra_ref, rr_ref, rf_ref,
    wx_ref, wb_ref, wc_ref, off_ref, spd_ref, gain_ref,
    out_ref,
    xo, bo, co, ro, hs, hr, ws, wr,
    cum_t, rate_t, fac_t, ecum_t,
    xc, bc, cc, yl, zs, gs,
    ts, tr, ls, lr, pre, pcl,
    ss, sl, yr, ylr, ypre, ypcl,
    zq, zql, zr, zlr,
    isd, ir, es, er,
    ys, yx,
    d_s, d_r, h_s, h_r, w_s, w_r,
    t_s, t_r, l_s, l_r, s_s, s_r, sl_s, sl_r,
    q_s, q_r, ql_s, ql_r, i_s, i_r, e_s, e_r, y_s, y_r,
):
    nx, ny, nz = sizes
    pairs = nx // 2
    xw, bw = pairs * PW, pairs * 2 * STATE
    x, c, z, y = (lax.axis_index(n) for n in ("x", "c", "z", "y"))
    first = c == 0
    partner = {"c": 1 - c}
    lin = (z * ny + y) * nx + x
    total_chips = nx * ny * nz
    has_prev, has_next = lin > 0, lin < total_chips - 1

    def chip(at):
        at = lax.rem(at + total_chips, total_chips)
        rest = at // nx
        return {"x": lax.rem(at, nx), "y": lax.rem(rest, ny), "z": rest // ny}

    target_exists = jnp.logical_or(
        jnp.logical_and(first, has_prev), jnp.logical_and(jnp.logical_not(first), has_next)
    )
    target = chip(jnp.where(first, lin - 1, lin + 1))

    barrier = pltpu.get_barrier_semaphore()

    def greet(device):
        pl.semaphore_signal(barrier, inc=1, device_id=device, device_id_type=MESH)

    greet(partner)

    @pl.loop(1, nx)
    def _(k):
        at = lax.rem(x + k, nx)
        greet({"x": at})
        greet({"x": at, "c": 1 - c})

    @pl.loop(1, ny)
    def _(k):
        greet({"y": lax.rem(y + k, ny)})

    @pl.loop(1, nz)
    def _(k):
        greet({"z": lax.rem(z + k, nz)})

    @pl.when(has_prev)
    def _():
        greet({**chip(lin - 1), "c": 1})

    @pl.when(has_next)
    def _():
        greet({**chip(lin + 1), "c": 0})

    group = 2 * x + c
    slot = lax.rem(group, nx)
    parity = lax.rem(slot, 2)
    place = (iota((GW, PW), 1) == iota((GW, PW), 0) + GW * parity).astype(BF16)
    ws[:, 0:PW] = mm(wx_ref[...], place).astype(BF16)
    ws[:, PW : PW + STATE] = wb_ref[...]
    ws[:, PW + STATE : PW + 2 * STATE] = wc_ref[...]
    lane = iota((1, 128), 1)
    base = 16 * (slot // 2) + HPG * parity
    tap = iota((TAPS, 128), 0)
    for k, ref in enumerate((off_ref, spd_ref)):
        row = jnp.zeros((1, 128), F32)
        for d in range(2):
            for i in range(HPG):
                row = jnp.where(lane == base + 8 * d + i, ref[d : d + 1, i : i + 1], row)
        parts = [v.astype(F32) for v in three(row)]
        rows = jnp.where(
            tap == 0, parts[0], jnp.where(tap == 1, parts[1], jnp.where(tap == 2, parts[2], 0.0))
        )
        lo = PW + (2 + k) * STATE
        ws[:, lo : lo + STATE] = rows.astype(BF16)

    at = 0
    for ref, width in ((x_ref, xw), (b_ref, bw), (c_ref, bw)):
        for half in range(2):
            cols = pl.ds(half * width, width)
            last = ref[0, TOK - 16 : TOK, cols].astype(F32)[8:16]
            start = ref[0, 0:16, cols].astype(F32)[0:8]
            rows = jnp.where(first, start, pltpu.roll(last, 2, 0))
            hs[half, :, at : at + width] = rows[0:2]
        at += width

    @pl.when(jnp.logical_not(has_prev))
    def _():
        hr[0] = jnp.zeros(hr.shape[1:], F32)

    @pl.when(jnp.logical_not(has_next))
    def _():
        hr[1] = jnp.zeros(hr.shape[1:], F32)

    expected = 1 + 2 * (nx - 1) + (ny - 1) + (nz - 1)
    pl.semaphore_wait(barrier, expected + jnp.where(target_exists, 2, 0))

    def half_of(ref, width, half):
        return ref.at[0, :, pl.ds(pl.multiple_of(half * width, 128), width)]

    rate_copies = [
        rcopy(ref.at[0], ro.at[k], d_s.at[k], d_r.at[k], partner)
        for k, ref in enumerate((ra_ref, rr_ref, rf_ref))
    ]
    data_copies = [
        rcopy(half_of(ref, width, 1 - c), dst, d_s.at[3 + k], d_r.at[3 + k], partner)
        for k, (ref, width, dst) in enumerate(((x_ref, xw, xo), (b_ref, bw, bo), (c_ref, bw, co)))
    ]

    to_core = group // nx

    def weight_copy(j):
        return rcopy(ws, wr.at[slot], w_s.at[j], w_r.at[slot], {"x": j, "c": to_core})

    def weight_is_mine(j):
        return jnp.logical_and(j == x, to_core == c)

    @pl.loop(0, nx)
    def _(k):
        j = lax.rem(x + nx // 2 + k, nx)

        @pl.when(jnp.logical_not(weight_is_mine(j)))
        def _():
            weight_copy(j).start()

    @pl.when(to_core == c)
    def _():
        wr[slot] = ws[...]

    for copy in rate_copies:
        copy.start()

    def halo_copy(half):
        return rcopy(
            hs.at[half], hr.at[1 - c], h_s.at[half], h_r.at[1 - c], {**target, "c": half}
        )

    @pl.when(target_exists)
    def _():
        for half in range(2):
            halo_copy(half).start()

    for copy in data_copies:
        copy.start()

    for copy in rate_copies:
        copy.wait_recv()

    n = 2 * TOK
    heads = ra_ref.shape[1]
    lanes, head = iota((128, heads), 0), iota((128, heads), 1)
    pair, rest = lanes // 16, lax.rem(lanes, 16)
    inside = lax.rem(rest, 8)
    valid = jnp.logical_and(inside < 6, pair < pairs)
    valid = jnp.logical_and(valid, head == 6 * pairs * c + 6 * pair + inside)
    pick_f = jnp.logical_and(valid, rest < 8).astype(F32)
    pick_b = jnp.logical_and(valid, rest >= 8).astype(F32)

    def both(ref, k):
        own, other = ref[0], ro[k]
        return jnp.concatenate(
            [jnp.where(first, own, other), jnp.where(first, other, own)], axis=1
        )

    raw = mm(pick_f, both(ra_ref, 0), HIGH) + mm(pick_b, both(rr_ref, 1), HIGH)
    fading = mm(pick_f + pick_b, both(rf_ref, 2), HIGH)

    @pl.loop(0, nx)
    def _(j):
        @pl.when(jnp.logical_not(nx * c + j == group))
        def _():
            rcopy(ws, wr.at[j], w_s.at[j], w_r.at[j], partner).wait_recv()

    def summed(lo):
        row = jnp.zeros((1, 128), F32)
        for j in range(nx):
            v = wr[j, :, lo : lo + 128].astype(F32)
            row = row + ((v[0:1] + v[1:2]) + v[2:3])
        return jnp.broadcast_to(row, (8, 128)).T[:, 0:1]

    offset, speed = summed(PW + 2 * STATE), summed(PW + 3 * STATE)
    pre_rate = raw + offset
    rate = jnp.maximum(pre_rate, 0.0) + jnp.log1p(jnp.exp(-jnp.abs(pre_rate)))
    log = fading - jnp.exp(speed) * rate
    row_i, col_i = iota((n, n), 0), iota((n, n), 1)
    forward = lax.rem(iota((128, 1), 0), 16) < 8
    upper, lower = (row_i <= col_i).astype(BF16), (row_i >= col_i).astype(BF16)
    parts = three(log)
    cum = jnp.where(
        forward,
        (mm(parts[2], upper) + mm(parts[1], upper)) + mm(parts[0], upper),
        (mm(parts[2], lower) + mm(parts[1], lower)) + mm(parts[0], lower),
    )
    span = jnp.where(forward, cum[:, n - 1 : n], cum[:, 0:1])
    cum_t[...] = cum
    rate_t[...] = rate
    fac_t[...] = rate * jnp.exp(span - cum)
    ecum_t[...] = jnp.exp(cum)

    @pl.when(has_prev)
    def _():
        rcopy(hs.at[0], hr.at[0], h_s.at[0], h_r.at[0], partner).wait_recv()

    @pl.when(has_next)
    def _():
        rcopy(hs.at[0], hr.at[1], h_s.at[0], h_r.at[1], partner).wait_recv()

    for copy in data_copies:
        copy.wait_recv()

    low = iota((1, 128), 1) < HEAD_DIM

    def rows_of(p):
        return pl.ds(pl.multiple_of(16 * p, 16), 16)

    def x_cols(p):
        return pl.ds(pl.multiple_of(PW * p, 128), PW)

    def b_cols(p):
        return pl.ds(pl.multiple_of(2 * STATE * p, 128), 2 * STATE)

    def state_copy(m, j):
        return rcopy(
            ts.at[m, j], tr.at[m, x], t_s.at[m * nx + j], t_r.at[m * nx + x], {"x": j}
        )

    def log_copy(j):
        return rcopy(ls.at[j], lr.at[x], l_s.at[j], l_r.at[x], {"x": j})

    def state_conv(p, own, other, at, lo):
        start = pl.multiple_of(2 * STATE * p, 128)
        taps = jnp.concatenate(
            [wr[2 * p, :, lo : lo + STATE], wr[2 * p + 1, :, lo : lo + STATE]], axis=1
        ).astype(F32)
        cols_in = pl.ds(pl.multiple_of(c * bw + start, 128), 2 * STATE)
        cols_h = pl.ds(pl.multiple_of(at + start, 128), 2 * STATE)
        return conv_silu(
            own[0, :, cols_in], other[:, b_cols(p)], hr[0, :, cols_h], hr[1, :, cols_h],
            taps, first,
        )

    @pl.loop(0, pairs)
    def _(k):
        p = lax.rem(x // 2 + 1 + k, pairs)
        w0, w1 = wr[2 * p].astype(F32), wr[2 * p + 1].astype(F32)
        cols, start = x_cols(p), pl.multiple_of(PW * p, 128)
        x_cols_in = pl.ds(pl.multiple_of(c * xw + start, 128), PW)
        xv = conv_silu(
            x_ref[0, :, x_cols_in], xo[:, cols], hr[0, :, cols], hr[1, :, cols],
            w0[:, 0:PW] + w1[:, 0:PW], first,
        )
        xc[:, cols] = xv
        bv = state_conv(p, b_ref, bo, xw, PW)
        bc[:, b_cols(p)] = bv
        factors = fac_t[rows_of(p)].T
        cums = cum_t[rows_of(p)].T
        direction = iota((1, 16), 1) < 8
        spans = jnp.where(direction, cums[n - 1 : n], cums[0:1])
        xf = xv.astype(F32)
        bf = bv.astype(F32)
        for q in range(2):
            j = 2 * p + q
            scaled, span_row = [], []
            for i in range(HPG):
                f, g = HPG * q + i, 8 + HPG * q + i
                v = xf[:, 128 * (f // 2) : 128 * (f // 2 + 1)]
                turned = pltpu.roll(v, HEAD_DIM, 1)
                twice = jnp.where(low, v, turned) if f % 2 == 0 else jnp.where(low, turned, v)
                scaled.append(twice * head_rows(factors, f, g))
                span_row.append(head_rows(spans, f, g))
            scaled = jnp.concatenate(scaled, axis=1)
            span_row = jnp.concatenate(span_row, axis=1)
            hi = scaled.astype(BF16)
            lo = (scaled - hi.astype(F32)).astype(BF16)
            bt = bf[:, q * STATE : (q + 1) * STATE].T.astype(BF16)
            update = (mm(bt, hi) + mm(bt, lo)).astype(BF16)

            @pl.when(j == x)
            def _():
                for m in range(HPG):
                    tr[m, x] = update[:, 128 * m : 128 * (m + 1)]
                lr[x] = span_row

            @pl.when(j != x)
            def _():
                ls[j] = span_row
                for m in range(HPG):
                    ts[m, j] = update[:, 128 * m : 128 * (m + 1)]
                log_copy(j).start()
                state_copy(0, j).start()

    for m in range(1, HPG):
        @pl.loop(1, nx)
        def _(k):
            state_copy(m, lax.rem(x + k, nx)).start()

    @pl.loop(0, pairs)
    def _(p):
        cum_r, rate_r = cum_t[rows_of(p)], rate_t[rows_of(p)]
        cum_c = cum_r.T
        cv = state_conv(p, c_ref, co, xw + bw, PW + STATE)
        cc[:, b_cols(p)] = cv
        xv, bv = xc[:, x_cols(p)], bc[:, b_cols(p)]
        below, above = col_i < row_i, col_i > row_i
        products = []
        for q in range(2):
            scores = lax.dot_general(
                cv[:, q * STATE : (q + 1) * STATE], bv[:, q * STATE : (q + 1) * STATE],
                (((1,), (1,)), ((), ())), preferred_element_type=F32,
            )
            for i in range(HPG):
                f, g = HPG * q + i, 8 + HPG * q + i
                gap = jnp.where(
                    above,
                    cum_c[:, g : g + 1] - cum_r[g : g + 1],
                    cum_c[:, f : f + 1] - cum_r[f : f + 1],
                )
                r_f, r_b = rate_r[f : f + 1], rate_r[g : g + 1]
                coef = jnp.where(below, r_f, jnp.where(above, r_b, r_f + r_b))
                weights = (scores * jnp.exp(gap) * coef).astype(BF16)
                v = f // 2
                products.append(mm(weights, xv[:, 128 * v : 128 * (v + 1)]))
        yl[:, x_cols(p)] = jnp.concatenate(
            [jnp.where(low, products[2 * v], products[2 * v + 1]) for v in range(HPG)], axis=1
        )

    def gate_cols(k):
        return pl.ds(pl.multiple_of(k * PW, 128), PW)

    ry = STATE // ny

    def y_rows(j):
        return pl.ds(pl.multiple_of(ry * j, ry), ry)

    def part(row, m):
        return row[:, 128 * m : 128 * (m + 1)]

    def along_x(m):
        @pl.loop(0, nx)
        def _(k):
            @pl.when(k != x)
            def _():
                if m == 0:
                    rcopy(ls.at[k], lr.at[k], l_s.at[k], l_r.at[k], partner).wait_recv()
                at = m * nx + k
                rcopy(ts.at[m, k], tr.at[m, k], t_s.at[at], t_r.at[at], partner).wait_recv()

        if m == 0:
            pcl[0] = jnp.zeros(pcl.shape[1:], F32)
            wide = jnp.concatenate([low] * HPG, axis=1)

            @pl.loop(0, nx)
            def _(k):
                pcl[k + 1] = pcl[k] + jnp.where(wide, lr[k], lr[nx - 1 - k])

            sl[...] = pcl[nx]

        pre[m, 0] = jnp.zeros(pre.shape[2:], F32)

        @pl.loop(0, nx)
        def _(k):
            d = jnp.where(low, part(lr[k], m), part(lr[nx - 1 - k], m))
            v = jnp.where(low, tr[m, k].astype(F32), tr[m, nx - 1 - k].astype(F32))
            pre[m, k + 1] = pre[m, k] * jnp.exp(d) + v

        ss[m] = pre[m, nx].astype(ss.dtype)

        @pl.loop(1, ny)
        def _(k):
            j = lax.rem(y + k, ny)
            if m == 0:
                rcopy(sl, ylr.at[y], sl_s.at[j], sl_r.at[y], {"y": j}).start()
            total_copy(m, j).start()

        yr[m, y] = ss[m, y_rows(y)]
        if m == 0:
            ylr[y] = sl[...]

    def total_copy(m, j):
        return rcopy(
            ss.at[m, y_rows(j)], yr.at[m, y], s_s.at[m * ny + j], s_r.at[m * ny + y], {"y": j}
        )

    def plane_copy(m, j):
        return rcopy(zq.at[m], zr.at[m, z], q_s.at[m * nz + j], q_r.at[m * nz + z], {"z": j})

    def incoming_copy(m, j):
        return rcopy(
            isd.at[m, j], ir.at[m, y_rows(y)], i_s.at[m * ny + j], i_r.at[m * ny + y], {"y": j}
        )

    def entry_copy(m, j):
        return rcopy(
            es.at[m, j], er.at[m, x], e_s.at[m * nx + j], e_r.at[m * nx + x], {"x": j}
        )

    def along_y(m):
        @pl.loop(1, ny)
        def _(k):
            j = lax.rem(y + k, ny)
            if m == 0:
                rcopy(sl, ylr.at[j], sl_s.at[j], sl_r.at[j], {"y": j}).wait_recv()
            at = m * ny + j
            rcopy(ss.at[m, y_rows(j)], yr.at[m, j], s_s.at[at], s_r.at[at], {"y": j}).wait_recv()

        if m == 0:
            ypcl[0] = jnp.zeros(ypcl.shape[1:], F32)
            wide = jnp.concatenate([low] * HPG, axis=1)

            @pl.loop(0, ny)
            def _(k):
                ypcl[k + 1] = ypcl[k] + jnp.where(wide, ylr[k], ylr[ny - 1 - k])

            zql[...] = ypcl[ny]

        ypre[m, 0] = jnp.zeros(ypre.shape[2:], F32)

        @pl.loop(0, ny)
        def _(k):
            d = jnp.where(low, part(ylr[k], m), part(ylr[ny - 1 - k], m))
            v = jnp.where(low, yr[m, k].astype(F32), yr[m, ny - 1 - k].astype(F32))
            ypre[m, k + 1] = ypre[m, k] * jnp.exp(d) + v

        zq[m] = ypre[m, ny]

        @pl.loop(1, nz)
        def _(k):
            j = lax.rem(z + k, nz)
            if m == 0:
                rcopy(zql, zlr.at[z], ql_s.at[j], ql_r.at[z], {"z": j}).start()
            plane_copy(m, j).start()

        zr[m, z] = zq[m]
        if m == 0:
            zlr[z] = zql[...]

    def along_z(m):
        @pl.loop(1, nz)
        def _(k):
            j = lax.rem(z + k, nz)
            if m == 0:
                rcopy(zql, zlr.at[j], ql_s.at[j], ql_r.at[j], {"z": j}).wait_recv()
            at = m * nz + j
            rcopy(zq.at[m], zr.at[m, j], q_s.at[at], q_r.at[at], {"z": j}).wait_recv()

        running = jnp.zeros((ry, 128), F32)
        entering = jnp.zeros((ry, 128), F32)
        wanted = jnp.where(low, z, nz - 1 - z)
        for k in range(nz):
            entering = jnp.where(wanted == k, running, entering)
            d = jnp.where(low, part(zlr[k], m), part(zlr[nz - 1 - k], m))
            v = jnp.where(low, zr[m, k], zr[m, nz - 1 - k])
            running = running * jnp.exp(d) + v

        def incoming(j):
            f = ypre[m, j] + jnp.exp(part(ypcl[j], m)) * entering
            b = ypre[m, ny - 1 - j] + jnp.exp(part(ypcl[ny - 1 - j], m)) * entering
            return jnp.where(low, f, b).astype(ir.dtype)

        @pl.loop(1, ny)
        def _(k):
            j = lax.rem(y + k, ny)
            isd[m, j] = incoming(j)
            incoming_copy(m, j).start()

        ir[m, y_rows(y)] = incoming(y)

    def back_along_x(m):
        @pl.loop(1, ny)
        def _(k):
            j = lax.rem(y + k, ny)
            at = m * ny + j
            rcopy(isd.at[m, j], ir.at[m, y_rows(j)], i_s.at[at], i_r.at[at], {"y": j}).wait_recv()

        def entry(j):
            here = ir[m].astype(F32)
            f = pre[m, j] + jnp.exp(part(pcl[j], m)) * here
            b = pre[m, nx - 1 - j] + jnp.exp(part(pcl[nx - 1 - j], m)) * here
            return jnp.where(low, f, b).astype(BF16)

        @pl.loop(1, nx)
        def _(k):
            j = lax.rem(x + k, nx)
            es[m, j] = entry(j)
            entry_copy(m, j).start()

        er[m, x] = entry(x)

    def pair_at(k):
        away = (k + 1) // 2
        return lax.rem(x // 2 + jnp.where(lax.rem(k, 2) == 1, away, pairs - away), pairs)

    def carried(m, p):
        cv = cc[:, b_cols(p)]
        decays = ecum_t[rows_of(p)].T
        for q in range(2):
            j = 2 * p + q
            f, g = HPG * q + m, 8 + HPG * q + m

            @pl.when(j != x)
            def _():
                at = m * nx + j
                rcopy(es.at[m, j], er.at[m, j], e_s.at[at], e_r.at[at], partner).wait_recv()

            v = mm(part(cv, q), er[m, j]) * head_rows(decays, f, g)
            v = v + pltpu.roll(v, HEAD_DIM, 1)
            mine = low if f % 2 == 0 else jnp.logical_not(low)
            cols = pl.ds(pl.multiple_of(PW * p + 128 * (f // 2), 128), 128)
            yl[:, cols] = yl[:, cols] + jnp.where(mine, v, 0.0)

    along_x(0)

    for k in range(2 * xw // 128):
        cols = slice(128 * k, 128 * (k + 1))
        gs[:, cols] = gain_ref[cols].astype(F32).reshape(1, 128)

    @pl.loop(0, 2 * pairs)
    def _(k):
        zz = z_ref[0, :, gate_cols(k)].astype(F32)
        zs[:, gate_cols(k)] = zz / (1.0 + jnp.exp(-zz))

    along_x(1)
    along_y(0)
    along_x(2)
    along_z(0)
    along_y(1)
    back_along_x(0)
    along_y(2)
    along_z(1)
    back_along_x(1)
    along_z(2)

    for copy in rate_copies + data_copies:
        copy.wait_send()

    @pl.when(target_exists)
    def _():
        for half in range(2):
            halo_copy(half).wait_send()

    @pl.loop(0, nx)
    def _(j):
        @pl.when(jnp.logical_not(weight_is_mine(j)))
        def _():
            weight_copy(j).wait_send()

        @pl.when(j != x)
        def _():
            log_copy(j).wait_send()
            for m in range(HPG):
                state_copy(m, j).wait_send()

    @pl.loop(1, ny)
    def _(k):
        j = lax.rem(y + k, ny)
        rcopy(sl, ylr.at[y], sl_s.at[j], sl_r.at[y], {"y": j}).wait_send()
        for m in range(HPG):
            total_copy(m, j).wait_send()

    @pl.loop(1, nz)
    def _(k):
        j = lax.rem(z + k, nz)
        rcopy(zql, zlr.at[z], ql_s.at[j], ql_r.at[z], {"z": j}).wait_send()
        for m in range(HPG):
            plane_copy(m, j).wait_send()

    back_along_x(2)

    @pl.loop(1, ny)
    def _(k):
        for m in range(HPG):
            incoming_copy(m, lax.rem(y + k, ny)).wait_send()

    for m in range(HPG - 1):
        @pl.loop(0, pairs)
        def _(k):
            carried(m, pair_at(k))

    @pl.loop(1, nx)
    def _(k):
        for m in range(HPG - 1):
            entry_copy(m, lax.rem(x + k, nx)).wait_send()

    block_r, block_c = iota((128, 128), 0) // HEAD_DIM, iota((128, 128), 1) // HEAD_DIM
    ones = (block_r == block_c).astype(BF16)

    def gate(mixed, cols):
        g = mixed.astype(F32) * zs[:, cols]
        sq = g * g
        hi = sq.astype(BF16)
        lo = (sq - hi.astype(F32)).astype(BF16)
        means = jnp.concatenate(
            [mm(part(hi, v), ones) + mm(part(lo, v), ones) for v in range(HPG)], axis=1
        ) * (1.0 / HEAD_DIM)
        normed = g * lax.rsqrt(means + 1e-06)
        out_ref[0, :, cols] = (normed * gs[:, cols]).astype(BF16)

    def own_cols(p, half):
        return pl.ds(pl.multiple_of(half * xw + PW * p, 128), PW)

    def mixed_copy(p):
        return rcopy(ys.at[p], yx.at[p], y_s.at[p], y_r.at[p], partner)

    def other_half(p):
        mixed_copy(p).wait_recv()
        gate(yx[p], own_cols(p, 1 - c))

    @pl.loop(0, pairs)
    def _(k):
        p = pair_at(k)
        carried(HPG - 1, p)
        mixed = yl[:, x_cols(p)]
        top, bottom = mixed[0:TOK].astype(BF16), mixed[TOK:n].astype(BF16)
        ys[p] = jnp.where(first, bottom, top)
        mixed_copy(p).start()
        gate(jnp.where(first, top, bottom), own_cols(p, c))

        @pl.when(k > 0)
        def _():
            other_half(pair_at(k - 1))

    other_half(pair_at(pairs - 1))

    @pl.loop(1, nx)
    def _(k):
        entry_copy(HPG - 1, lax.rem(x + k, nx)).wait_send()

    @pl.loop(0, pairs)
    def _(p):
        mixed_copy(p).wait_send()


def local(sizes, *args):
    nx, ny, nz = sizes
    pairs = nx // 2
    xw, bw = pairs * PW, pairs * 2 * STATE
    n = 2 * TOK
    ry = STATE // ny
    args = list(args)
    args[4:7] = [jnp.swapaxes(a, 1, 2) for a in args[4:7]]
    dma = pltpu.SemaphoreType.DMA
    vmem = pltpu.VMEM
    wide = PW + 4 * STATE
    scratch = [
        vmem((TOK, xw), BF16), vmem((TOK, bw), BF16), vmem((TOK, bw), BF16),
        vmem((3, args[4].shape[1], TOK), F32),
        vmem((2, 2, xw + 2 * bw), F32), vmem((2, 2, xw + 2 * bw), F32),
        vmem((TAPS, wide), BF16), vmem((nx, TAPS, wide), BF16),
        vmem((128, n), F32), vmem((128, n), F32), vmem((128, n), F32), vmem((128, n), F32),
        vmem((n, xw), BF16), vmem((n, bw), BF16), vmem((n, bw), BF16), vmem((n, xw), F32),
        vmem((TOK, 2 * xw), F32), vmem((1, 2 * xw), F32),
        vmem((HPG, nx, STATE, 128), BF16), vmem((HPG, nx, STATE, 128), BF16),
        vmem((nx, 1, PW), F32), vmem((nx, 1, PW), F32),
        vmem((HPG, nx + 1, STATE, 128), F32), vmem((nx + 1, 1, PW), F32),
        vmem((HPG, STATE, 128), BF16), vmem((1, PW), F32),
        vmem((HPG, ny, ry, 128), BF16), vmem((ny, 1, PW), F32),
        vmem((HPG, ny + 1, ry, 128), F32), vmem((ny + 1, 1, PW), F32),
        vmem((HPG, ry, 128), F32), vmem((1, PW), F32),
        vmem((HPG, nz, ry, 128), F32), vmem((nz, 1, PW), F32),
        vmem((HPG, ny, ry, 128), BF16), vmem((HPG, STATE, 128), BF16),
        vmem((HPG, nx, STATE, 128), BF16), vmem((HPG, nx, STATE, 128), BF16),
        vmem((pairs, TOK, PW), BF16), vmem((pairs, TOK, PW), BF16),
    ]
    hx, hy, hz = HPG * nx, HPG * ny, HPG * nz
    counts = [6, 6, 2, 2, nx, nx, hx, hx, nx, nx, hy, hy, ny, ny, hz, hz, nz, nz, hy, hy, hx, hx, pairs, pairs]
    scratch += [dma((k,)) for k in counts]
    return pl.pallas_call(
        functools.partial(kernel, sizes),
        out_shape=jax.ShapeDtypeStruct(args[0].shape, BF16),
        in_specs=[pl.BlockSpec(memory_space=pltpu.VMEM)] * len(args),
        out_specs=pl.BlockSpec(memory_space=pltpu.VMEM),
        scratch_shapes=scratch,
        compiler_params=pltpu.CompilerParams(
            collective_id=0, has_side_effects=True, vmem_limit_bytes=60 * 1024 * 1024
        ),
        name="mixer",
    )(*args)


def solution(mesh):
    sp, dp = mesh.shape["sp"], mesh.shape["dp"]
    nx = sp // 2
    ny = max(k for k in range(1, dp + 1) if dp % k == 0 and k * k <= dp)
    nz = dp // ny
    torus = Mesh(mesh.devices.reshape(nx, 2, nz, ny), ("x", "c", "z", "y"))
    rows = P(("z", "y"), ("x", "c"), None)
    cols = P(None, ("x", "c"))
    return jax.shard_map(
        functools.partial(local, (nx, ny, nz)),
        mesh=torus,
        in_specs=(rows,) * 7 + (cols,) * 5 + (P(),),
        out_specs=rows,
        check_vma=False,
    )
```

time: 102 us -> 86.4 us (0.85)
  Pallas kernels: 95.8 us -> 84.1 us
  local copies, waits for them, and re-layouts: 6.29 us -> 2.06 us
    pallas_call x1, Pallas kernels: 95.8 us -> 84.1 us  [local(): pl.pallas_call(functools.partial(kernel, sizes), out_shape=jax.ShapeDtype...]
    unnamed x8 -> x1, local copies, waits for them, and re-layouts: 5 us -> 2.06 us
    broadcast_in_dim x1 -> x0, local copies, waits for them, and re-layouts: 1.29 us -> none  [local(): args = args[:-1] + (args[-1][None],)]
where the time goes in v1:
time: 86.4 us; the launch traced here: 86.1 us
  Pallas kernels  84.1 us (97%)
  local copies, waits for them, and re-layouts  2.06 us (2%)
    pallas_call x1, Pallas kernels, local(): pl.pallas_call(functools.partial(kernel, sizes), out_shape=jax.ShapeDtype...  84.1 us
    unnamed x1, local copies, waits for them, and re-layouts  2.06 us

profile of v1, /device:TPU:1, one launch (start us, length us, event | category | flops | bytes accessed | tf_op | source)
XLA Modules:
  0.0 86.1 jit_solution(7194338140358907827)
XLA Ops:
  0.0 84.1 %mixer.1 = bf16[1,128,3072]{2,1,0:T(8,128)(2,1)} custom-call(bf16[1,128,3072]{2,1,0:T(8,128)(2,1)} %x_ref.1, bf16[1,128,2048]{2,1,0:T(8,128)(2,1)} %b_ref.1, bf16[1,128,2048]{2,1,0:T(8,128)(2,1)} %c_ref.1, bf16[1,128,3072]{2,1,0:T(8,128)(2,1)} %z_ref.1, f32[1,48,128]{2,1,0:T(8,128)} %bitcast.3, f32[1,48,128]{2,1,0:T(8,128)} %bitcast.4, ...), custom_call_target="tpu_custom_call" | custom-call | tf_op jit(solution)/shard_map/mixer/pallas_call | solution.py:749
  84.1 2.1 %copy.15 = bf16[1,128,3072]{2,1,0:T(8,128)(2,1)} copy(bf16[1,128,3072]{2,1,0:T(8,128)(2,1)} %mixer.1) | data formatting | bytes 1572864

commit v2 on v1

--- a/solution.py
+++ b/solution.py
@@ -45,20 +45,22 @@
     return jnp.where(low, columns[:, f : f + 1], columns[:, b : b + 1])
 
 
+def silu(t):
+    h = 0.5 * t
+    return h + h * jnp.tanh(h)
+
+
 def conv_silu(own, other, before, after, taps, first):
-    own, other = own.astype(F32), other.astype(F32)
-    x = jnp.concatenate(
-        [jnp.where(first, own, other), jnp.where(first, other, own)], axis=0
-    )
+    top, bottom = jnp.where(first, own, other), jnp.where(first, other, own)
+    edge = iota((8, own.shape[1]), 0)
+    ahead = jnp.where(edge == 6, before[0:1], jnp.where(edge == 7, before[1:2], 0.0))
+    behind = jnp.where(edge == 0, after[0:1], 0.0)
+    x = jnp.concatenate([ahead, top.astype(F32), bottom.astype(F32), behind], axis=0)
     rows = x.shape[0]
-    row = iota(x.shape, 0)
-    m1 = jnp.where(row == 0, before[1:2], pltpu.roll(x, 1, 0))
-    m2 = jnp.where(
-        row == 0, before[0:1], jnp.where(row == 1, before[1:2], pltpu.roll(x, 2, 0))
-    )
-    p1 = jnp.where(row == rows - 1, after[0:1], pltpu.roll(x, rows - 1, 0))
-    total = m2 * taps[0:1] + m1 * taps[1:2] + x * taps[2:3] + p1 * taps[3:4]
-    return (total / (1.0 + jnp.exp(-total))).astype(BF16)
+    inner = slice(8, rows - 8)
+    m2, m1, p1 = (pltpu.roll(x, k, 0)[inner] for k in (2, 1, rows - 1))
+    total = m2 * taps[0:1] + m1 * taps[1:2] + x[inner] * taps[2:3] + p1 * taps[3:4]
+    return silu(total).astype(BF16)
 
 
 def three(v):
@@ -70,11 +72,13 @@
 
 def kernel(
     sizes,
+    x_in, b_in, c_in, z_in, ra_in, rr_in, rf_in,
+    wx_in, wb_in, wc_in, off_in, spd_in, gain_in,
+    out_ref,
     x_ref, b_ref, c_ref, z_ref, ra_ref, rr_ref, rf_ref,
-    wx_ref, wb_ref, wc_ref, off_ref, spd_ref, gain_ref,
-    out_ref,
+    wx_ref, wb_ref, wc_ref, off_ref, spd_ref, gain_ref, in_s,
     xo, bo, co, ro, hs, hr, ws, wr,
-    cum_t, rate_t, fac_t, ecum_t,
+    cum_t, rate_t, fac_t, ecum_t, span_row_of,
     xc, bc, cc, yl, zs, gs,
     ts, tr, ls, lr, pre, pcl,
     ss, sl, yr, ylr, ypre, ypcl,
@@ -85,6 +89,20 @@
     t_s, t_r, l_s, l_r, s_s, s_r, sl_s, sl_r,
     q_s, q_r, ql_s, ql_r, i_s, i_r, e_s, e_r, y_s, y_r,
 ):
+    sources = (
+        wx_in, wb_in, wc_in, off_in, spd_in, x_in, b_in, c_in, ra_in, rr_in, rf_in, z_in, gain_in
+    )
+    places = (
+        wx_ref, wb_ref, wc_ref, off_ref, spd_ref, x_ref, b_ref, c_ref, ra_ref, rr_ref, rf_ref,
+        z_ref, gain_ref,
+    )
+    loads = [
+        pltpu.make_async_copy(source, place, in_s.at[k])
+        for k, (source, place) in enumerate(zip(sources, places))
+    ]
+    for load in loads:
+        load.start()
+
     nx, ny, nz = sizes
     pairs = nx // 2
     xw, bw = pairs * PW, pairs * 2 * STATE
@@ -133,6 +151,9 @@
     @pl.when(has_next)
     def _():
         greet({**chip(lin + 1), "c": 0})
+
+    for load in loads[:5]:
+        load.wait()
 
     group = 2 * x + c
     slot = lax.rem(group, nx)
@@ -156,6 +177,9 @@
         lo = PW + (2 + k) * STATE
         ws[:, lo : lo + STATE] = rows.astype(BF16)
 
+    for load in loads[5:8]:
+        load.wait()
+
     at = 0
     for ref, width in ((x_ref, xw), (b_ref, bw), (c_ref, bw)):
         for half in range(2):
@@ -174,6 +198,9 @@
     def _():
         hr[1] = jnp.zeros(hr.shape[1:], F32)
 
+    for load in loads[8:]:
+        load.wait()
+
     expected = 1 + 2 * (nx - 1) + (ny - 1) + (nz - 1)
     pl.semaphore_wait(barrier, expected + jnp.where(target_exists, 2, 0))
 
@@ -246,6 +273,18 @@
 
     raw = mm(pick_f, both(ra_ref, 0), HIGH) + mm(pick_b, both(rr_ref, 1), HIGH)
     fading = mm(pick_f + pick_b, both(rf_ref, 2), HIGH)
+
+    def gate_cols(k):
+        return pl.ds(pl.multiple_of(k * PW, 128), PW)
+
+    for k in range(2 * xw // 128):
+        cols = slice(128 * k, 128 * (k + 1))
+        gs[:, cols] = gain_ref[cols].astype(F32).reshape(1, 128)
+
+    @pl.loop(0, 2 * pairs)
+    def _(k):
+        zz = z_ref[0, :, gate_cols(k)].astype(F32)
+        zs[:, gate_cols(k)] = silu(zz)
 
     @pl.loop(0, nx)
     def _(j):
@@ -274,6 +313,9 @@
         (mm(parts[2], lower) + mm(parts[1], lower)) + mm(parts[0], lower),
     )
     span = jnp.where(forward, cum[:, n - 1 : n], cum[:, 0:1])
+    span_line = jnp.broadcast_to(span, (128, 128)).T[0:1]
+    for p in range(pairs):
+        span_row_of[p] = span_line[:, 16 * p : 16 * (p + 1)]
     cum_t[...] = cum
     rate_t[...] = rate
     fac_t[...] = rate * jnp.exp(span - cum)
@@ -301,10 +343,26 @@
     def b_cols(p):
         return pl.ds(pl.multiple_of(2 * STATE * p, 128), 2 * STATE)
 
-    def state_copy(m, j):
+    half_rows = STATE // 2
+    chunks = 2 * HPG
+
+    def rows_in(u):
+        return pl.ds(half_rows * (u % 2), half_rows)
+
+    def state_copy(u, j):
         return rcopy(
-            ts.at[m, j], tr.at[m, x], t_s.at[m * nx + j], t_r.at[m * nx + x], {"x": j}
-        )
+            ts.at[u // 2, j, rows_in(u)], tr.at[u // 2, x, rows_in(u)],
+            t_s.at[u * nx + j], t_r.at[u * nx + x], {"x": j},
+        )
+
+    def send_state(u, p):
+        for q in range(2):
+            @pl.when(2 * p + q != x)
+            def _():
+                state_copy(u, 2 * p + q).start()
+
+    def conv_pair(k):
+        return lax.rem(x // 2 + 1 + k, pairs)
 
     def log_copy(j):
         return rcopy(ls.at[j], lr.at[x], l_s.at[j], l_r.at[x], {"x": j})
@@ -323,7 +381,7 @@
 
     @pl.loop(0, pairs)
     def _(k):
-        p = lax.rem(x // 2 + 1 + k, pairs)
+        p = conv_pair(k)
         w0, w1 = wr[2 * p].astype(F32), wr[2 * p + 1].astype(F32)
         cols, start = x_cols(p), pl.multiple_of(PW * p, 128)
         x_cols_in = pl.ds(pl.multiple_of(c * xw + start, 128), PW)
@@ -334,47 +392,49 @@
         xc[:, cols] = xv
         bv = state_conv(p, b_ref, bo, xw, PW)
         bc[:, b_cols(p)] = bv
-        factors = fac_t[rows_of(p)].T
-        cums = cum_t[rows_of(p)].T
-        direction = iota((1, 16), 1) < 8
-        spans = jnp.where(direction, cums[n - 1 : n], cums[0:1])
-        xf = xv.astype(F32)
+        factors, spans = fac_t[rows_of(p)], span_row_of[p]
         bf = bv.astype(F32)
         for q in range(2):
             j = 2 * p + q
-            scaled, span_row = [], []
+            bt = bf[:, q * STATE : (q + 1) * STATE].T
+            update, span_row = [], []
             for i in range(HPG):
                 f, g = HPG * q + i, 8 + HPG * q + i
-                v = xf[:, 128 * (f // 2) : 128 * (f // 2 + 1)]
-                turned = pltpu.roll(v, HEAD_DIM, 1)
-                twice = jnp.where(low, v, turned) if f % 2 == 0 else jnp.where(low, turned, v)
-                scaled.append(twice * head_rows(factors, f, g))
+                v = xv[:, 128 * (f // 2) : 128 * (f // 2 + 1)]
+                ahead = mm((bt * factors[f : f + 1]).astype(BF16), v)
+                back = mm((bt * factors[g : g + 1]).astype(BF16), v)
+                if f % 2 == 0:
+                    both_ways = jnp.where(low, ahead, pltpu.roll(back, HEAD_DIM, 1))
+                else:
+                    both_ways = jnp.where(low, pltpu.roll(ahead, HEAD_DIM, 1), back)
+                update.append(both_ways.astype(BF16))
                 span_row.append(head_rows(spans, f, g))
-            scaled = jnp.concatenate(scaled, axis=1)
             span_row = jnp.concatenate(span_row, axis=1)
-            hi = scaled.astype(BF16)
-            lo = (scaled - hi.astype(F32)).astype(BF16)
-            bt = bf[:, q * STATE : (q + 1) * STATE].T.astype(BF16)
-            update = (mm(bt, hi) + mm(bt, lo)).astype(BF16)
 
             @pl.when(j == x)
             def _():
                 for m in range(HPG):
-                    tr[m, x] = update[:, 128 * m : 128 * (m + 1)]
+                    tr[m, x] = update[m]
                 lr[x] = span_row
 
             @pl.when(j != x)
             def _():
                 ls[j] = span_row
                 for m in range(HPG):
-                    ts[m, j] = update[:, 128 * m : 128 * (m + 1)]
+                    ts[m, j] = update[m]
                 log_copy(j).start()
-                state_copy(0, j).start()
-
-    for m in range(1, HPG):
+
+        send_state(0, p)
+
+        @pl.when(k > 0)
+        def _():
+            send_state(1, conv_pair(k - 1))
+
+    send_state(1, conv_pair(pairs - 1))
+    for u in range(2, chunks):
         @pl.loop(1, nx)
         def _(k):
-            state_copy(m, lax.rem(x + k, nx)).start()
+            state_copy(u, lax.rem(x + k, nx)).start()
 
     @pl.loop(0, pairs)
     def _(p):
@@ -406,28 +466,26 @@
             [jnp.where(low, products[2 * v], products[2 * v + 1]) for v in range(HPG)], axis=1
         )
 
-    def gate_cols(k):
-        return pl.ds(pl.multiple_of(k * PW, 128), PW)
-
-    ry = STATE // ny
-
-    def y_rows(j):
-        return pl.ds(pl.multiple_of(ry * j, ry), ry)
+    ry = half_rows // ny
 
     def part(row, m):
         return row[:, 128 * m : 128 * (m + 1)]
 
-    def along_x(m):
+    def along_x(u):
+        m, rows = u // 2, rows_in(u)
+
         @pl.loop(0, nx)
         def _(k):
             @pl.when(k != x)
             def _():
-                if m == 0:
+                if u == 0:
                     rcopy(ls.at[k], lr.at[k], l_s.at[k], l_r.at[k], partner).wait_recv()
-                at = m * nx + k
-                rcopy(ts.at[m, k], tr.at[m, k], t_s.at[at], t_r.at[at], partner).wait_recv()
-
-        if m == 0:
+                at = u * nx + k
+                rcopy(
+                    ts.at[m, k, rows], tr.at[m, k, rows], t_s.at[at], t_r.at[at], partner
+                ).wait_recv()
+
+        if u == 0:
             pcl[0] = jnp.zeros(pcl.shape[1:], F32)
             wide = jnp.concatenate([low] * HPG, axis=1)
 
@@ -437,55 +495,58 @@
 
             sl[...] = pcl[nx]
 
-        pre[m, 0] = jnp.zeros(pre.shape[2:], F32)
+        pre[m, 0, rows] = jnp.zeros((half_rows, 128), F32)
 
         @pl.loop(0, nx)
         def _(k):
             d = jnp.where(low, part(lr[k], m), part(lr[nx - 1 - k], m))
-            v = jnp.where(low, tr[m, k].astype(F32), tr[m, nx - 1 - k].astype(F32))
-            pre[m, k + 1] = pre[m, k] * jnp.exp(d) + v
-
-        ss[m] = pre[m, nx].astype(ss.dtype)
+            v = jnp.where(low, tr[m, k, rows].astype(F32), tr[m, nx - 1 - k, rows].astype(F32))
+            pre[m, k + 1, rows] = pre[m, k, rows] * jnp.exp(d) + v
+
+        ss[u] = pre[m, nx, rows].reshape(ny, ry, 128).astype(ss.dtype)
 
         @pl.loop(1, ny)
         def _(k):
             j = lax.rem(y + k, ny)
-            if m == 0:
+            if u == 0:
                 rcopy(sl, ylr.at[y], sl_s.at[j], sl_r.at[y], {"y": j}).start()
-            total_copy(m, j).start()
-
-        yr[m, y] = ss[m, y_rows(y)]
-        if m == 0:
+            total_copy(u, j).start()
+
+        yr[u, y] = ss[u, y]
+        if u == 0:
             ylr[y] = sl[...]
 
-    def total_copy(m, j):
+    def total_copy(u, j):
         return rcopy(
-            ss.at[m, y_rows(j)], yr.at[m, y], s_s.at[m * ny + j], s_r.at[m * ny + y], {"y": j}
-        )
-
-    def plane_copy(m, j):
-        return rcopy(zq.at[m], zr.at[m, z], q_s.at[m * nz + j], q_r.at[m * nz + z], {"z": j})
-
-    def incoming_copy(m, j):
+            ss.at[u, j], yr.at[u, y], s_s.at[u * ny + j], s_r.at[u * ny + y], {"y": j}
+        )
+
+    def plane_copy(u, j):
+        return rcopy(zq.at[u], zr.at[u, z], q_s.at[u * nz + j], q_r.at[u * nz + z], {"z": j})
+
+    def incoming_copy(u, j):
         return rcopy(
-            isd.at[m, j], ir.at[m, y_rows(y)], i_s.at[m * ny + j], i_r.at[m * ny + y], {"y": j}
-        )
-
-    def entry_copy(m, j):
+            isd.at[u, j], ir.at[u, y], i_s.at[u * ny + j], i_r.at[u * ny + y], {"y": j}
+        )
+
+    def entry_copy(u, j):
         return rcopy(
-            es.at[m, j], er.at[m, x], e_s.at[m * nx + j], e_r.at[m * nx + x], {"x": j}
-        )
-
-    def along_y(m):
+            es.at[u // 2, j, rows_in(u)], er.at[u // 2, x, rows_in(u)],
+            e_s.at[u * nx + j], e_r.at[u * nx + x], {"x": j},
+        )
+
+    def along_y(u):
+        m = u // 2
+
         @pl.loop(1, ny)
         def _(k):
             j = lax.rem(y + k, ny)
-            if m == 0:
+            if u == 0:
                 rcopy(sl, ylr.at[j], sl_s.at[j], sl_r.at[j], {"y": j}).wait_recv()
-            at = m * ny + j
-            rcopy(ss.at[m, y_rows(j)], yr.at[m, j], s_s.at[at], s_r.at[at], {"y": j}).wait_recv()
-
-        if m == 0:
+            at = u * ny + j
+            rcopy(ss.at[u, j], yr.at[u, j], s_s.at[at], s_r.at[at], {"y": j}).wait_recv()
+
+        if u == 0:
             ypcl[0] = jnp.zeros(ypcl.shape[1:], F32)
             wide = jnp.concatenate([low] * HPG, axis=1)
 
@@ -495,35 +556,35 @@
 
             zql[...] = ypcl[ny]
 
-        ypre[m, 0] = jnp.zeros(ypre.shape[2:], F32)
-
-        @pl.loop(0, ny)
-        def _(k):
+        running = jnp.zeros((ry, 128), F32)
+        for k in range(ny):
+            ypre[u, k] = running
             d = jnp.where(low, part(ylr[k], m), part(ylr[ny - 1 - k], m))
-            v = jnp.where(low, yr[m, k].astype(F32), yr[m, ny - 1 - k].astype(F32))
-            ypre[m, k + 1] = ypre[m, k] * jnp.exp(d) + v
-
-        zq[m] = ypre[m, ny]
+            v = jnp.where(low, yr[u, k].astype(F32), yr[u, ny - 1 - k].astype(F32))
+            running = running * jnp.exp(d) + v
+        zq[u] = running
 
         @pl.loop(1, nz)
         def _(k):
             j = lax.rem(z + k, nz)
-            if m == 0:
+            if u == 0:
                 rcopy(zql, zlr.at[z], ql_s.at[j], ql_r.at[z], {"z": j}).start()
-            plane_copy(m, j).start()
-
-        zr[m, z] = zq[m]
-        if m == 0:
+            plane_copy(u, j).start()
+
+        zr[u, z] = zq[u]
+        if u == 0:
             zlr[z] = zql[...]
 
-    def along_z(m):
+    def along_z(u):
+        m = u // 2
+
         @pl.loop(1, nz)
         def _(k):
             j = lax.rem(z + k, nz)
-            if m == 0:
+            if u == 0:
                 rcopy(zql, zlr.at[j], ql_s.at[j], ql_r.at[j], {"z": j}).wait_recv()
-            at = m * nz + j
-            rcopy(zq.at[m], zr.at[m, j], q_s.at[at], q_r.at[at], {"z": j}).wait_recv()
+            at = u * nz + j
+            rcopy(zq.at[u], zr.at[u, j], q_s.at[at], q_r.at[at], {"z": j}).wait_recv()
 
         running = jnp.zeros((ry, 128), F32)
         entering = jnp.zeros((ry, 128), F32)
@@ -531,137 +592,139 @@
         for k in range(nz):
             entering = jnp.where(wanted == k, running, entering)
             d = jnp.where(low, part(zlr[k], m), part(zlr[nz - 1 - k], m))
-            v = jnp.where(low, zr[m, k], zr[m, nz - 1 - k])
+            v = jnp.where(low, zr[u, k], zr[u, nz - 1 - k])
             running = running * jnp.exp(d) + v
 
         def incoming(j):
-            f = ypre[m, j] + jnp.exp(part(ypcl[j], m)) * entering
-            b = ypre[m, ny - 1 - j] + jnp.exp(part(ypcl[ny - 1 - j], m)) * entering
+            f = ypre[u, j] + jnp.exp(part(ypcl[j], m)) * entering
+            b = ypre[u, ny - 1 - j] + jnp.exp(part(ypcl[ny - 1 - j], m)) * entering
             return jnp.where(low, f, b).astype(ir.dtype)
 
         @pl.loop(1, ny)
         def _(k):
             j = lax.rem(y + k, ny)
-            isd[m, j] = incoming(j)
-            incoming_copy(m, j).start()
-
-        ir[m, y_rows(y)] = incoming(y)
-
-    def back_along_x(m):
+            isd[u, j] = incoming(j)
+            incoming_copy(u, j).start()
+
+        ir[u, y] = incoming(y)
+
+    def back_along_x(u):
+        m, rows = u // 2, rows_in(u)
+
         @pl.loop(1, ny)
         def _(k):
             j = lax.rem(y + k, ny)
-            at = m * ny + j
-            rcopy(isd.at[m, j], ir.at[m, y_rows(j)], i_s.at[at], i_r.at[at], {"y": j}).wait_recv()
+            at = u * ny + j
+            rcopy(isd.at[u, j], ir.at[u, j], i_s.at[at], i_r.at[at], {"y": j}).wait_recv()
+
+        here = ir[u].astype(F32).reshape(half_rows, 128)
 
         def entry(j):
-            here = ir[m].astype(F32)
-            f = pre[m, j] + jnp.exp(part(pcl[j], m)) * here
-            b = pre[m, nx - 1 - j] + jnp.exp(part(pcl[nx - 1 - j], m)) * here
+            f = pre[m, j, rows] + jnp.exp(part(pcl[j], m)) * here
+            b = pre[m, nx - 1 - j, rows] + jnp.exp(part(pcl[nx - 1 - j], m)) * here
             return jnp.where(low, f, b).astype(BF16)
 
         @pl.loop(1, nx)
         def _(k):
             j = lax.rem(x + k, nx)
-            es[m, j] = entry(j)
-            entry_copy(m, j).start()
-
-        er[m, x] = entry(x)
+            es[m, j, rows] = entry(j)
+            entry_copy(u, j).start()
+
+        er[m, x, rows] = entry(x)
 
     def pair_at(k):
         away = (k + 1) // 2
         return lax.rem(x // 2 + jnp.where(lax.rem(k, 2) == 1, away, pairs - away), pairs)
+
+    def await_entries(m, p):
+        for q in range(2):
+            j = 2 * p + q
+
+            @pl.when(j != x)
+            def _():
+                for u in (2 * m, 2 * m + 1):
+                    at, rows = u * nx + j, rows_in(u)
+                    rcopy(
+                        es.at[m, j, rows], er.at[m, j, rows], e_s.at[at], e_r.at[at], partner
+                    ).wait_recv()
 
     def carried(m, p):
         cv = cc[:, b_cols(p)]
         decays = ecum_t[rows_of(p)].T
         for q in range(2):
-            j = 2 * p + q
             f, g = HPG * q + m, 8 + HPG * q + m
-
-            @pl.when(j != x)
-            def _():
-                at = m * nx + j
-                rcopy(es.at[m, j], er.at[m, j], e_s.at[at], e_r.at[at], partner).wait_recv()
-
-            v = mm(part(cv, q), er[m, j]) * head_rows(decays, f, g)
+            v = mm(part(cv, q), er[m, 2 * p + q]) * head_rows(decays, f, g)
             v = v + pltpu.roll(v, HEAD_DIM, 1)
             mine = low if f % 2 == 0 else jnp.logical_not(low)
             cols = pl.ds(pl.multiple_of(PW * p + 128 * (f // 2), 128), 128)
             yl[:, cols] = yl[:, cols] + jnp.where(mine, v, 0.0)
 
-    along_x(0)
-
-    for k in range(2 * xw // 128):
-        cols = slice(128 * k, 128 * (k + 1))
-        gs[:, cols] = gain_ref[cols].astype(F32).reshape(1, 128)
-
-    @pl.loop(0, 2 * pairs)
-    def _(k):
-        zz = z_ref[0, :, gate_cols(k)].astype(F32)
-        zs[:, gate_cols(k)] = zz / (1.0 + jnp.exp(-zz))
-
-    along_x(1)
-    along_y(0)
-    along_x(2)
-    along_z(0)
-    along_y(1)
-    back_along_x(0)
-    along_y(2)
-    along_z(1)
-    back_along_x(1)
-    along_z(2)
-
-    for copy in rate_copies + data_copies:
-        copy.wait_send()
-
-    @pl.when(target_exists)
-    def _():
-        for half in range(2):
-            halo_copy(half).wait_send()
-
-    @pl.loop(0, nx)
-    def _(j):
-        @pl.when(jnp.logical_not(weight_is_mine(j)))
+    def free_sends():
+        for copy in rate_copies + data_copies:
+            copy.wait_send()
+
+        @pl.when(target_exists)
         def _():
-            weight_copy(j).wait_send()
-
-        @pl.when(j != x)
-        def _():
-            log_copy(j).wait_send()
-            for m in range(HPG):
-                state_copy(m, j).wait_send()
+            for half in range(2):
+                halo_copy(half).wait_send()
+
+        @pl.loop(0, nx)
+        def _(j):
+            @pl.when(jnp.logical_not(weight_is_mine(j)))
+            def _():
+                weight_copy(j).wait_send()
+
+            @pl.when(j != x)
+            def _():
+                log_copy(j).wait_send()
+                for m in range(chunks):
+                    state_copy(m, j).wait_send()
+
+        @pl.loop(1, ny)
+        def _(k):
+            j = lax.rem(y + k, ny)
+            rcopy(sl, ylr.at[y], sl_s.at[j], sl_r.at[y], {"y": j}).wait_send()
+            for m in range(chunks):
+                total_copy(m, j).wait_send()
+
+        @pl.loop(1, nz)
+        def _(k):
+            j = lax.rem(z + k, nz)
+            rcopy(zql, zlr.at[z], ql_s.at[j], ql_r.at[z], {"z": j}).wait_send()
+            for m in range(chunks):
+                plane_copy(m, j).wait_send()
+
+    def carry(m):
+        @pl.loop(0, pairs)
+        def _(k):
+            await_entries(m, pair_at(k))
+
+        @pl.loop(0, pairs)
+        def _(p):
+            carried(m, p)
+
+    arrival, stage = 2.9, 5.3
+    steps = []
+    for u in range(chunks):
+        for k, step in enumerate((along_x, along_y, along_z, back_along_x)):
+            steps.append((arrival * u + stage * k, step, u))
+    steps.append((arrival + 3 * stage + 9.5, carry, 0))
+    for _, step, u in sorted(steps, key=lambda t: t[0]):
+        if step is back_along_x and u == chunks - 1:
+            free_sends()
+        step(u)
 
     @pl.loop(1, ny)
     def _(k):
-        j = lax.rem(y + k, ny)
-        rcopy(sl, ylr.at[y], sl_s.at[j], sl_r.at[y], {"y": j}).wait_send()
-        for m in range(HPG):
-            total_copy(m, j).wait_send()
-
-    @pl.loop(1, nz)
-    def _(k):
-        j = lax.rem(z + k, nz)
-        rcopy(zql, zlr.at[z], ql_s.at[j], ql_r.at[z], {"z": j}).wait_send()
-        for m in range(HPG):
-            plane_copy(m, j).wait_send()
-
-    back_along_x(2)
-
-    @pl.loop(1, ny)
-    def _(k):
-        for m in range(HPG):
+        for m in range(chunks):
             incoming_copy(m, lax.rem(y + k, ny)).wait_send()
 
-    for m in range(HPG - 1):
-        @pl.loop(0, pairs)
-        def _(k):
-            carried(m, pair_at(k))
+    carry(1)
 
     @pl.loop(1, nx)
     def _(k):
-        for m in range(HPG - 1):
-            entry_copy(m, lax.rem(x + k, nx)).wait_send()
+        for u in range(2 * (HPG - 1)):
+            entry_copy(u, lax.rem(x + k, nx)).wait_send()
 
     block_r, block_c = iota((128, 128), 0) // HEAD_DIM, iota((128, 128), 1) // HEAD_DIM
     ones = (block_r == block_c).astype(BF16)
@@ -690,6 +753,7 @@
     @pl.loop(0, pairs)
     def _(k):
         p = pair_at(k)
+        await_entries(HPG - 1, p)
         carried(HPG - 1, p)
         mixed = yl[:, x_cols(p)]
         top, bottom = mixed[0:TOK].astype(BF16), mixed[TOK:n].astype(BF16)
@@ -705,7 +769,8 @@
 
     @pl.loop(1, nx)
     def _(k):
-        entry_copy(HPG - 1, lax.rem(x + k, nx)).wait_send()
+        for u in (chunks - 2, chunks - 1):
+            entry_copy(u, lax.rem(x + k, nx)).wait_send()
 
     @pl.loop(0, pairs)
     def _(p):
@@ -717,39 +782,42 @@
     pairs = nx // 2
     xw, bw = pairs * PW, pairs * 2 * STATE
     n = 2 * TOK
-    ry = STATE // ny
+    ry = STATE // 2 // ny
+    chunks = 2 * HPG
     args = list(args)
     args[4:7] = [jnp.swapaxes(a, 1, 2) for a in args[4:7]]
     dma = pltpu.SemaphoreType.DMA
     vmem = pltpu.VMEM
     wide = PW + 4 * STATE
-    scratch = [
+    scratch = [vmem(a.shape, a.dtype) for a in args] + [dma((len(args),))]
+    scratch += [
         vmem((TOK, xw), BF16), vmem((TOK, bw), BF16), vmem((TOK, bw), BF16),
         vmem((3, args[4].shape[1], TOK), F32),
         vmem((2, 2, xw + 2 * bw), F32), vmem((2, 2, xw + 2 * bw), F32),
         vmem((TAPS, wide), BF16), vmem((nx, TAPS, wide), BF16),
         vmem((128, n), F32), vmem((128, n), F32), vmem((128, n), F32), vmem((128, n), F32),
+        vmem((pairs, 1, 16), F32),
         vmem((n, xw), BF16), vmem((n, bw), BF16), vmem((n, bw), BF16), vmem((n, xw), F32),
         vmem((TOK, 2 * xw), F32), vmem((1, 2 * xw), F32),
         vmem((HPG, nx, STATE, 128), BF16), vmem((HPG, nx, STATE, 128), BF16),
         vmem((nx, 1, PW), F32), vmem((nx, 1, PW), F32),
         vmem((HPG, nx + 1, STATE, 128), F32), vmem((nx + 1, 1, PW), F32),
-        vmem((HPG, STATE, 128), BF16), vmem((1, PW), F32),
-        vmem((HPG, ny, ry, 128), BF16), vmem((ny, 1, PW), F32),
-        vmem((HPG, ny + 1, ry, 128), F32), vmem((ny + 1, 1, PW), F32),
-        vmem((HPG, ry, 128), F32), vmem((1, PW), F32),
-        vmem((HPG, nz, ry, 128), F32), vmem((nz, 1, PW), F32),
-        vmem((HPG, ny, ry, 128), BF16), vmem((HPG, STATE, 128), BF16),
+        vmem((chunks, ny, ry, 128), BF16), vmem((1, PW), F32),
+        vmem((chunks, ny, ry, 128), BF16), vmem((ny, 1, PW), F32),
+        vmem((chunks, ny, ry, 128), F32), vmem((ny + 1, 1, PW), F32),
+        vmem((chunks, ry, 128), F32), vmem((1, PW), F32),
+        vmem((chunks, nz, ry, 128), F32), vmem((nz, 1, PW), F32),
+        vmem((chunks, ny, ry, 128), BF16), vmem((chunks, ny, ry, 128), BF16),
         vmem((HPG, nx, STATE, 128), BF16), vmem((HPG, nx, STATE, 128), BF16),
         vmem((pairs, TOK, PW), BF16), vmem((pairs, TOK, PW), BF16),
     ]
-    hx, hy, hz = HPG * nx, HPG * ny, HPG * nz
+    hx, hy, hz = chunks * nx, chunks * ny, chunks * nz
     counts = [6, 6, 2, 2, nx, nx, hx, hx, nx, nx, hy, hy, ny, ny, hz, hz, nz, nz, hy, hy, hx, hx, pairs, pairs]
     scratch += [dma((k,)) for k in counts]
     return pl.pallas_call(
         functools.partial(kernel, sizes),
-        out_shape=jax.ShapeDtypeStruct(args[0].shape, BF16),
-        in_specs=[pl.BlockSpec(memory_space=pltpu.VMEM)] * len(args),
+        out_shape=pltpu.VMEM(args[0].shape, BF16),
+        in_specs=[pl.BlockSpec(memory_space=pltpu.HBM)] * len(args),
         out_specs=pl.BlockSpec(memory_space=pltpu.VMEM),
         scratch_shapes=scratch,
         compiler_params=pltpu.CompilerParams(

time: 86.4 us -> 80 us (0.926)
  Pallas kernels: 84.1 us -> 78.9 us
  local copies, waits for them, and re-layouts: 2.06 us -> 0.88 us
    pallas_call x1, Pallas kernels: 84.1 us -> 78.9 us  [local(): pl.pallas_call(functools.partial(kernel, sizes), out_shape=pltpu.VMEM(arg...]
    unnamed x1, local copies, waits for them, and re-layouts: 2.06 us -> 0.88 us
where the time goes in v2:
time: 80 us; the launch traced here: 79.8 us
  Pallas kernels  78.9 us (99%)
  local copies, waits for them, and re-layouts  0.88 us (1%)
    pallas_call x1, Pallas kernels, local(): pl.pallas_call(functools.partial(kernel, sizes), out_shape=pltpu.VMEM(arg...  78.9 us

profile of v2, /device:TPU:1, one launch (start us, length us, event | category | flops | bytes accessed | tf_op | source)
XLA Modules:
  0.0 79.8 jit_solution(5065085482533958102)
XLA Ops:
  0.0 78.9 %mixer.1 = bf16[1,128,3072]{2,1,0:T(8,128)(2,1)S(1)} custom-call(bf16[1,128,3072]{2,1,0:T(8,128)(2,1)} %x_in.1, bf16[1,128,2048]{2,1,0:T(8,128)(2,1)} %b_in.1, bf16[1,128,2048]{2,1,0:T(8,128)(2,1)} %c_in.1, bf16[1,128,3072]{2,1,0:T(8,128)(2,1)} %z_in.1, f32[1,48,128]{2,1,0:T(8,128)} %bitcast.3, f32[1,48,128]{2,1,0:T(8,128)} %bitcast.4, ...), custom_call_target="tpu_custom_call" | custom-call | tf_op jit(solution)/shard_map/mixer/pallas_call | solution.py:817
  78.9 0.9 %copy.15 = bf16[1,128,3072]{2,1,0:T(8,128)(2,1)} copy(bf16[1,128,3072]{2,1,0:T(8,128)(2,1)S(1)} %mixer.1) | data formatting | bytes 1572864

commit v3 on v2

--- a/solution.py
+++ b/solution.py
@@ -78,7 +78,7 @@
     x_ref, b_ref, c_ref, z_ref, ra_ref, rr_ref, rf_ref,
     wx_ref, wb_ref, wc_ref, off_ref, spd_ref, gain_ref, in_s,
     xo, bo, co, ro, hs, hr, ws, wr,
-    cum_t, rate_t, fac_t, ecum_t, span_row_of,
+    cum_t, rate_t, fac_t, ecum_t, span_row_of, bts,
     xc, bc, cc, yl, zs, gs,
     ts, tr, ls, lr, pre, pcl,
     ss, sl, yr, ylr, ypre, ypcl,
@@ -355,12 +355,6 @@
             t_s.at[u * nx + j], t_r.at[u * nx + x], {"x": j},
         )
 
-    def send_state(u, p):
-        for q in range(2):
-            @pl.when(2 * p + q != x)
-            def _():
-                state_copy(u, 2 * p + q).start()
-
     def conv_pair(k):
         return lax.rem(x // 2 + 1 + k, pairs)
 
@@ -379,6 +373,19 @@
             taps, first,
         )
 
+    def own_state(p, q, i, bt):
+        j, factors = 2 * p + q, fac_t[rows_of(p)]
+        f, g = HPG * q + i, 8 + HPG * q + i
+        cols = pl.ds(pl.multiple_of(PW * p + 128 * (f // 2), 128), 128)
+        v = xc[:, cols]
+        ahead = mm((bt * factors[f : f + 1]).astype(BF16), v)
+        back = mm((bt * factors[g : g + 1]).astype(BF16), v)
+        if f % 2 == 0:
+            update = jnp.where(low, ahead, pltpu.roll(back, HEAD_DIM, 1))
+        else:
+            update = jnp.where(low, pltpu.roll(ahead, HEAD_DIM, 1), back)
+        ts[i, j] = update.astype(BF16)
+
     @pl.loop(0, pairs)
     def _(k):
         p = conv_pair(k)
@@ -392,52 +399,47 @@
         xc[:, cols] = xv
         bv = state_conv(p, b_ref, bo, xw, PW)
         bc[:, b_cols(p)] = bv
-        factors, spans = fac_t[rows_of(p)], span_row_of[p]
         bf = bv.astype(F32)
         for q in range(2):
-            j = 2 * p + q
             bt = bf[:, q * STATE : (q + 1) * STATE].T
-            update, span_row = [], []
-            for i in range(HPG):
-                f, g = HPG * q + i, 8 + HPG * q + i
-                v = xv[:, 128 * (f // 2) : 128 * (f // 2 + 1)]
-                ahead = mm((bt * factors[f : f + 1]).astype(BF16), v)
-                back = mm((bt * factors[g : g + 1]).astype(BF16), v)
-                if f % 2 == 0:
-                    both_ways = jnp.where(low, ahead, pltpu.roll(back, HEAD_DIM, 1))
-                else:
-                    both_ways = jnp.where(low, pltpu.roll(ahead, HEAD_DIM, 1), back)
-                update.append(both_ways.astype(BF16))
-                span_row.append(head_rows(spans, f, g))
-            span_row = jnp.concatenate(span_row, axis=1)
-
-            @pl.when(j == x)
+            bts[2 * p + q] = bt
+            own_state(p, q, 0, bt)
+            ls[2 * p + q] = jnp.concatenate(
+                [
+                    head_rows(span_row_of[p], HPG * q + i, 8 + HPG * q + i)
+                    for i in range(HPG)
+                ],
+                axis=1,
+            )
+        for q in range(2):
+            @pl.when(2 * p + q != x)
             def _():
-                for m in range(HPG):
-                    tr[m, x] = update[m]
-                lr[x] = span_row
-
-            @pl.when(j != x)
-            def _():
-                ls[j] = span_row
-                for m in range(HPG):
-                    ts[m, j] = update[m]
-                log_copy(j).start()
-
-        send_state(0, p)
-
-        @pl.when(k > 0)
-        def _():
-            send_state(1, conv_pair(k - 1))
-
-    send_state(1, conv_pair(pairs - 1))
+                log_copy(2 * p + q).start()
+                state_copy(0, 2 * p + q).start()
+
+    lr[x] = ls[x]
+
+    def send_chunk(u):
+        @pl.loop(1, nx)
+        def _(k):
+            state_copy(u, lax.rem(x + k, nx)).start()
+
+    send_chunk(1)
+
+    @pl.loop(0, pairs)
+    def _(k):
+        p = conv_pair(k)
+        for q in range(2):
+            bt = bts[2 * p + q]
+            for i in range(1, HPG):
+                own_state(p, q, i, bt)
+
     for u in range(2, chunks):
-        @pl.loop(1, nx)
-        def _(k):
-            state_copy(u, lax.rem(x + k, nx)).start()
-
-    @pl.loop(0, pairs)
-    def _(p):
+        send_chunk(u)
+    for m in range(HPG):
+        tr[m, x] = ts[m, x]
+
+    def inside_chip(p):
         cum_r, rate_r = cum_t[rows_of(p)], rate_t[rows_of(p)]
         cum_c = cum_r.T
         cv = state_conv(p, c_ref, co, xw + bw, PW + STATE)
@@ -704,7 +706,15 @@
             carried(m, p)
 
     arrival, stage = 2.9, 5.3
+    early = (pairs + 1) // 2
     steps = []
+
+    @pl.loop(0, early)
+    def _(p):
+        inside_chip(p)
+
+    for k, p in enumerate(range(early, pairs)):
+        steps.append((0.4 + arrival * k, inside_chip, p))
     for u in range(chunks):
         for k, step in enumerate((along_x, along_y, along_z, back_along_x)):
             steps.append((arrival * u + stage * k, step, u))
@@ -796,7 +806,7 @@
         vmem((2, 2, xw + 2 * bw), F32), vmem((2, 2, xw + 2 * bw), F32),
         vmem((TAPS, wide), BF16), vmem((nx, TAPS, wide), BF16),
         vmem((128, n), F32), vmem((128, n), F32), vmem((128, n), F32), vmem((128, n), F32),
-        vmem((pairs, 1, 16), F32),
+        vmem((pairs, 1, 16), F32), vmem((nx, STATE, n), F32),
         vmem((n, xw), BF16), vmem((n, bw), BF16), vmem((n, bw), BF16), vmem((n, xw), F32),
         vmem((TOK, 2 * xw), F32), vmem((1, 2 * xw), F32),
         vmem((HPG, nx, STATE, 128), BF16), vmem((HPG, nx, STATE, 128), BF16),

time: 80 us -> 78.6 us (0.982)
  Pallas kernels: 78.9 us -> 77.5 us
    pallas_call x1, Pallas kernels: 78.9 us -> 77.5 us  [local(): pl.pallas_call(functools.partial(kernel, sizes), out_shape=pltpu.VMEM(arg...]
where the time goes in v3:
time: 78.6 us; the launch traced here: 78.4 us
  Pallas kernels  77.5 us (99%)
  local copies, waits for them, and re-layouts  0.88 us (1%)
    pallas_call x1, Pallas kernels, local(): pl.pallas_call(functools.partial(kernel, sizes), out_shape=pltpu.VMEM(arg...  77.5 us

profile of v3, /device:TPU:1, one launch (start us, length us, event | category | flops | bytes accessed | tf_op | source)
XLA Modules:
  0.0 78.4 jit_solution(14830608562754529672)
XLA Ops:
  0.0 77.5 %mixer.1 = bf16[1,128,3072]{2,1,0:T(8,128)(2,1)S(1)} custom-call(bf16[1,128,3072]{2,1,0:T(8,128)(2,1)} %x_in.1, bf16[1,128,2048]{2,1,0:T(8,128)(2,1)} %b_in.1, bf16[1,128,2048]{2,1,0:T(8,128)(2,1)} %c_in.1, bf16[1,128,3072]{2,1,0:T(8,128)(2,1)} %z_in.1, f32[1,48,128]{2,1,0:T(8,128)} %bitcast.3, f32[1,48,128]{2,1,0:T(8,128)} %bitcast.4, ...), custom_call_target="tpu_custom_call" | custom-call | tf_op jit(solution)/shard_map/mixer/pallas_call | solution.py:827
  77.6 0.9 %copy.15 = bf16[1,128,3072]{2,1,0:T(8,128)(2,1)} copy(bf16[1,128,3072]{2,1,0:T(8,128)(2,1)S(1)} %mixer.1) | data formatting | bytes 1572864
